TPU v7x, 128 devices: a whole 4x4x4 slice. The times are simulated.
128 devices in a mesh: sp: 16 (over z, y), dp: 8 (over x, core).
Axes of the slice: x: 4, y: 4, z: 4, core: 2. Of those that a mesh axis runs over, the one named last changes fastest.
Arguments:
- query_nope: bfloat16 [8, 4096, 16, 128], P('dp', 'sp'), may hold values from -6 to 6
- query_rope: bfloat16 [8, 4096, 16, 64], P('dp', 'sp'), may hold values from -160 to 160
- latent: bfloat16 [8, 4096, 256], P('dp', 'sp'), may hold values from -6 to 6
- key_rope: bfloat16 [8, 4096, 64], P('dp', 'sp'), may hold values from -4 to 4
- resid: bfloat16 [8, 4096, 2048], P('dp', 'sp'), may hold values from -6 to 6
- latent_gain: float32 [256], replicated, may hold values from 0.1 to 1.9
- key_up: bfloat16 [256, 2048], P(None, 'sp'), may hold values from -0.375 to 0.375
- value_up: bfloat16 [256, 2048], P(None, 'sp'), may hold values from -0.375 to 0.375
- out_proj: bfloat16 [2048, 2048], P('sp', 'dp'), may hold values from -0.125 to 0.125
- norm_gain: float32 [2048], replicated, may hold values from 0.1 to 1.9
- expert_gate: bfloat16 [16, 2048, 1024], P('sp'), may hold values from -0.125 to 0.125
- expert_up: bfloat16 [16, 2048, 1024], P('sp'), may hold values from -0.125 to 0.125
- expert_down: bfloat16 [16, 1024, 2048], P('sp'), may hold values from -0.1875 to 0.1875
- routes: int32 [8, 4096, 2], P('dp', 'sp'), may hold values from 0 to 15, all different within a row; in each aligned block of 256 rows (0 to 255, 256 to 511, ..., all dimensions but the last counted through in order) at most 64 rows name the same one
- route_weight: float32 [8, 4096, 2], P('dp', 'sp'), may hold values from 0.2 to 1
Outputs:
- mixed: bfloat16 [8, 4096, 2048], P('dp', 'sp')
Inputs may be any that keep to these rules, and one draw needn't show every extreme that they name: `routes`: each token names two different experts. Among the tokens of one device no expert is named more than 64 times, and in every draw some expert is named exactly 64 times by some device's tokens.
All inputs are finite; a program needn't handle non-finite values.
Results may differ from a plain program's by a relative error of at most 0.0075.
Values may be sent and summed in bfloat16 or wider, within the bound.
A program may use at most 128 MiB of HBM per device.

v0:
```python
import jax
import jax.numpy as jnp
from jax import lax
from jax.sharding import PartitionSpec as P

epsilon = 1e-06
rope_base = 10000.0
masked_score = -1e30


def sent_together(arrays, axis, dim, along):
    both = jnp.concatenate(arrays, axis=along)
    out, at, finished = (lax.all_gather(both, axis, axis=dim, tiled=True), 0, [])
    for a in arrays:
        finished.append(lax.slice_in_dim(out, at, at + a.shape[along], axis=along))
        at += a.shape[along]
    return tuple(finished)


def rotate(values, positions):
    half_width = values.shape[-1] // 2
    frequency = rope_base ** (-jnp.arange(half_width, dtype=jnp.float32) / half_width)
    angles = positions.astype(jnp.float32)[:, None] * frequency[None, :]
    cosine = jnp.cos(angles)
    sine_part = jnp.sin(angles)
    if values.ndim == 3:
        cosine = cosine[:, None, :]
        sine_part = sine_part[:, None, :]
    floats = values.astype(jnp.float32)
    first_half = floats[..., :half_width]
    second_half = floats[..., half_width:]
    turned = jnp.concatenate(
        [
            first_half * cosine - second_half * sine_part,
            second_half * cosine + first_half * sine_part,
        ],
        axis=-1,
    )
    return turned.astype(jnp.bfloat16)


def rms_scaled(values, gain):
    floats = values.astype(jnp.float32)
    return floats * lax.rsqrt(jnp.mean(floats * floats, axis=-1, keepdims=True) + epsilon) * gain


def assign_slots(route_block, experts_all, capacity):
    flat_routes = route_block.reshape(-1)
    onehot = (flat_routes[:, None] == jnp.arange(experts_all, dtype=jnp.int32)[None, :]).astype(
        jnp.int32
    )
    earlier = jnp.cumsum(onehot, axis=0) - onehot
    placed = jnp.sum(earlier * onehot, axis=1)
    return flat_routes * capacity + placed


def fill_slots(rows, slot_ids, experts_all, capacity):
    pairs = slot_ids.shape[0]
    matches = jnp.arange(experts_all * capacity, dtype=jnp.int32)[:, None] == slot_ids[None, :]
    source = (
        jnp.sum(jnp.where(matches, jnp.arange(pairs, dtype=jnp.int32)[None, :], 0), axis=1) // 2
    )
    filled = jnp.any(matches, axis=1)
    picked = jnp.take(rows, source, axis=0)
    chosen = jnp.where(filled[:, None], picked, jnp.zeros_like(picked))
    return chosen.reshape(experts_all, capacity, rows.shape[-1])


def combine_slots(returned, slot_ids, weights):
    flat_back = returned.reshape(-1, returned.shape[-1])
    picked = (
        jnp.take(flat_back, slot_ids, axis=0).astype(jnp.float32).reshape(weights.shape[0], 2, -1)
    )
    return jnp.sum(weights[:, :, None] * picked, axis=1)


def shards(
    query_nope,
    query_rope,
    latent,
    key_rope,
    resid,
    latent_gain,
    key_up,
    value_up,
    out_proj,
    norm_gain,
    expert_gate,
    expert_up,
    expert_down,
    routes,
    route_weight,
):
    tokens_here = latent.shape[1]
    sp_count = lax.axis_size("sp")
    length = tokens_here * sp_count
    block = min(512, length)
    blocks = length // block
    local_pos = lax.axis_index("sp") * tokens_here + jnp.arange(tokens_here, dtype=jnp.int32)
    latent_normed = rms_scaled(latent[0], latent_gain).astype(jnp.bfloat16)
    key_turned = rotate(key_rope[0], local_pos)
    query_turned = rotate(query_rope[0], local_pos)
    all_latent, all_keyturn = sent_together((latent_normed, key_turned), "sp", 0, 1)
    query_plain, query_turn = (
        lax.all_to_all(query_nope[0], "sp", split_axis=1, concat_axis=0, tiled=True),
        lax.all_to_all(query_turned, "sp", split_axis=1, concat_axis=0, tiled=True),
    )
    heads_here = query_plain.shape[1]
    key_plain = (
        jnp.dot(all_latent, key_up, preferred_element_type=jnp.float32)
        .astype(jnp.bfloat16)
        .reshape(length, heads_here, -1)
    )
    value_heads = (
        jnp.dot(all_latent, value_up, preferred_element_type=jnp.float32)
        .astype(jnp.bfloat16)
        .reshape(length, heads_here, -1)
    )
    scale = (query_plain.shape[-1] + query_turn.shape[-1]) ** (-0.5)
    key_ids = jnp.arange(length, dtype=jnp.int32)

    def one_block(items):
        index, plain_block, turn_block = items
        scores = jnp.einsum(
            "bhd,shd->hbs", plain_block, key_plain, preferred_element_type=jnp.float32
        )
        scores = (
            scores
            + jnp.einsum("bhr,sr->hbs", turn_block, all_keyturn, preferred_element_type=jnp.float32)
        ) * scale
        row_ids = index * block + jnp.arange(block, dtype=jnp.int32)
        allowed = key_ids[None, :] <= row_ids[:, None]
        scores = jnp.where(allowed[None], scores, masked_score)
        largest = jnp.max(scores, axis=-1, keepdims=True)
        powers = jnp.exp(scores - largest)
        attend = (powers / jnp.sum(powers, axis=-1, keepdims=True)).astype(jnp.bfloat16)
        return jnp.einsum(
            "hbs,shd->bhd", attend, value_heads, preferred_element_type=jnp.float32
        ).astype(jnp.bfloat16)

    attended = lax.map(
        one_block,
        (
            jnp.arange(blocks, dtype=jnp.int32),
            query_plain.reshape(blocks, block, heads_here, -1),
            query_turn.reshape(blocks, block, heads_here, -1),
        ),
    )
    attended = attended.reshape(length, heads_here, -1)
    token_heads = lax.all_to_all(attended, "sp", split_axis=0, concat_axis=1, tiled=True)
    flat_heads = token_heads.reshape(tokens_here, -1)
    head_rows = lax.all_gather(out_proj, "dp", axis=1, tiled=True)
    projected = jnp.dot(
        flat_heads,
        lax.all_gather(head_rows, "sp", axis=0, tiled=True),
        preferred_element_type=jnp.float32,
    ).astype(jnp.bfloat16)
    after_attention = resid[0].astype(jnp.float32) + projected.astype(jnp.float32)
    normed = rms_scaled(after_attention, norm_gain).astype(jnp.bfloat16)
    experts_all = sp_count * expert_gate.shape[0]
    capacity = 4 * tokens_here // experts_all
    slot_ids = assign_slots(routes[0], experts_all, capacity)
    outgoing = fill_slots(normed, slot_ids, experts_all, capacity)
    arrived = lax.all_to_all(outgoing, "sp", split_axis=0, concat_axis=0, tiled=True)
    senders, slots_now, width = arrived.shape
    rows = arrived.reshape(senders * slots_now, width)
    gate = jnp.dot(rows, expert_gate[0], preferred_element_type=jnp.float32)
    upward = jnp.dot(rows, expert_up[0], preferred_element_type=jnp.float32)
    hidden = (jax.nn.silu(gate) * upward).astype(jnp.bfloat16)
    result = jnp.dot(hidden, expert_down[0], preferred_element_type=jnp.float32).astype(
        jnp.bfloat16
    )
    returned = lax.all_to_all(
        result.reshape(senders, slots_now, width), "sp", split_axis=0, concat_axis=0, tiled=True
    )
    routed = combine_slots(returned, slot_ids, route_weight[0])
    return (after_attention + routed).astype(jnp.bfloat16)[None]


def solution(mesh):
    return jax.shard_map(
        shards,
        mesh=mesh,
        in_specs=(
            P("dp", "sp", None, None),
            P("dp", "sp", None, None),
            P("dp", "sp", None),
            P("dp", "sp", None),
            P("dp", "sp", None),
            P(),
            P(None, "sp"),
            P(None, "sp"),
            P("sp", "dp"),
            P(),
            P("sp", None, None),
            P("sp", None, None),
            P("sp", None, None),
            P("dp", "sp", None),
            P("dp", "sp", None),
        ),
        out_specs=P("dp", "sp", None),
        check_vma=False,
    )
```

profile of v0, /device:TPU:0, one launch (start us, length us, event | category | flops | bytes accessed | tf_op | source)
XLA Modules:
  0.0 364.7 jit_solution(57491541784497012)
XLA Ops:
  12.9 8.2 %all-to-all-start.1 = ((bf16[256,16,64]{0,2,1:T(8,128)(2,1)}), bf16[256,16,64]{0,2,1:T(8,128)(2,1)S(1)}, u32[]{:S(2)}, u32[]{:S(2)}) async-start(bf16[256,16,64]{0,2,1:T(8,128)(2,1)} %pad_maximum_fusion), calls=%async_computation.1 | async-start | bytes 1048576 | tf_op jit(solution)/shard_map/all_to_all | solution.py:106
  22.3 12.0 %all-to-all-done.1 = bf16[256,16,64]{0,2,1:T(8,128)(2,1)S(1)} async-done(((bf16[256,16,64]{0,2,1:T(8,128)(2,1)}), bf16[256,16,64]{0,2,1:T(8,128)(2,1)S(1)}, u32[]{:S(2)}, u32[]{:S(2)}) %all-to-all-start.1) | async-done | bytes 524320 | tf_op jit(solution)/shard_map/all_to_all | solution.py:106
  38.0 14.6 %all_gather.10 = bf16[128,2048]{1,0:T(8,128)(2,1)} all-gather(bf16[128,256]{1,0:T(8,128)(2,1)S(1)} %copy-done.5), channel_id=1, replica_groups=mesh['sp'=16,'dp'=8] {'dp'}, dimensions={1}, use_global_device_ids=true | all-gather | bytes 589824 | tf_op jit(solution)/shard_map/all_gather | solution.py:152
  56.1 9.0 %all-gather.3.cloned.1.call-done = bf16[4096,320]{1,0:T(8,128)(2,1)} async-done(((bf16[256,320]{1,0:T(8,128)(2,1)}), bf16[4096,320]{1,0:T(8,128)(2,1)}) %all-gather.3.cloned.1.call-update) | async-done | bytes 2621456 | tf_op jit(solution)/shard_map/all_gather | solution.py:13
  70.7 82.8 %while.11 = (s32[]{:T(128)}, bf16[8,512,1,128]{3,1,2,0:T(8,128)(2,1)}, s32[8]{0:T(128)S(1)}, bf16[8,512,1,128]{3,1,2,0:T(8,128)(2,1)S(1)}, bf16[4096,1,128]{2,0,...) while((s32[]{:T(128)}, ...), condition=%wide.region_4.5_spmd.clone, body=%wide.region_1.4_spmd.clone.sunk | while | flops 1363213824 | bytes 49101984 | solution.py:141
  83.4 3.8 %fusion.77 = (f32[512]{0:T(512)S(1)}, f32[1,512,4096]{2,1,0:T(8,128)S(1)}) fusion(bf16[4096,64]{1,0:T(8,128)(2,1)S(1)} %get-tuple-element.234, bf16[8,512,1,64]{1,3,2,0:T(8,128)(2,1)} %get-tuple-element.233, s32[]{:T(128)} %get-tuple-element.218, f32[512,4096]{1,0:T(8,128)S(1)} %fusion.76, s32[512]{0:T(512)S(1)} %iota_add_fusion.2), kind=kOutput, calls=%fused_computation.103.clone.1 | convolution fusion | flops 278920704 | bytes 17371648 | tf_op jit(solution)/shard_map/while/body/eval_jaxpr/bhr,sr->hbs/dot_general | solution.py:129
  93.8 3.8 %fusion.77 = (f32[512]{0:T(512)S(1)}, f32[1,512,4096]{2,1,0:T(8,128)S(1)}) fusion(bf16[4096,64]{1,0:T(8,128)(2,1)S(1)} %get-tuple-element.234, bf16[8,512,1,64]{1,3,2,0:T(8,128)(2,1)} %get-tuple-element.233, s32[]{:T(128)} %get-tuple-element.218, f32[512,4096]{1,0:T(8,128)S(1)} %fusion.76, s32[512]{0:T(512)S(1)} %iota_add_fusion.2), kind=kOutput, calls=%fused_computation.103.clone.1 | convolution fusion | flops 278920704 | bytes 17371648 | tf_op jit(solution)/shard_map/while/body/eval_jaxpr/bhr,sr->hbs/dot_general | solution.py:129
  104.1 3.8 %fusion.77 = (f32[512]{0:T(512)S(1)}, f32[1,512,4096]{2,1,0:T(8,128)S(1)}) fusion(bf16[4096,64]{1,0:T(8,128)(2,1)S(1)} %get-tuple-element.234, bf16[8,512,1,64]{1,3,2,0:T(8,128)(2,1)} %get-tuple-element.233, s32[]{:T(128)} %get-tuple-element.218, f32[512,4096]{1,0:T(8,128)S(1)} %fusion.76, s32[512]{0:T(512)S(1)} %iota_add_fusion.2), kind=kOutput, calls=%fused_computation.103.clone.1 | convolution fusion | flops 278920704 | bytes 17371648 | tf_op jit(solution)/shard_map/while/body/eval_jaxpr/bhr,sr->hbs/dot_general | solution.py:129
  114.5 3.8 %fusion.77 = (f32[512]{0:T(512)S(1)}, f32[1,512,4096]{2,1,0:T(8,128)S(1)}) fusion(bf16[4096,64]{1,0:T(8,128)(2,1)S(1)} %get-tuple-element.234, bf16[8,512,1,64]{1,3,2,0:T(8,128)(2,1)} %get-tuple-element.233, s32[]{:T(128)} %get-tuple-element.218, f32[512,4096]{1,0:T(8,128)S(1)} %fusion.76, s32[512]{0:T(512)S(1)} %iota_add_fusion.2), kind=kOutput, calls=%fused_computation.103.clone.1 | convolution fusion | flops 278920704 | bytes 17371648 | tf_op jit(solution)/shard_map/while/body/eval_jaxpr/bhr,sr->hbs/dot_general | solution.py:129
  124.9 3.8 %fusion.77 = (f32[512]{0:T(512)S(1)}, f32[1,512,4096]{2,1,0:T(8,128)S(1)}) fusion(bf16[4096,64]{1,0:T(8,128)(2,1)S(1)} %get-tuple-element.234, bf16[8,512,1,64]{1,3,2,0:T(8,128)(2,1)} %get-tuple-element.233, s32[]{:T(128)} %get-tuple-element.218, f32[512,4096]{1,0:T(8,128)S(1)} %fusion.76, s32[512]{0:T(512)S(1)} %iota_add_fusion.2), kind=kOutput, calls=%fused_computation.103.clone.1 | convolution fusion | flops 278920704 | bytes 17371648 | tf_op jit(solution)/shard_map/while/body/eval_jaxpr/bhr,sr->hbs/dot_general | solution.py:129
  145.6 3.8 %fusion.77 = (f32[512]{0:T(512)S(1)}, f32[1,512,4096]{2,1,0:T(8,128)S(1)}) fusion(bf16[4096,64]{1,0:T(8,128)(2,1)S(1)} %get-tuple-element.234, bf16[8,512,1,64]{1,3,2,0:T(8,128)(2,1)} %get-tuple-element.233, s32[]{:T(128)} %get-tuple-element.218, f32[512,4096]{1,0:T(8,128)S(1)} %fusion.76, s32[512]{0:T(512)S(1)} %iota_add_fusion.2), kind=kOutput, calls=%fused_computation.103.clone.1 | convolution fusion | flops 278920704 | bytes 17371648 | tf_op jit(solution)/shard_map/while/body/eval_jaxpr/bhr,sr->hbs/dot_general | solution.py:129
  157.7 4.8 %all-to-all-start.2 = ((bf16[16,2,16384]{2,1,0:T(2,128)(2,1)}), bf16[16,2,16384]{2,1,0:T(2,128)(2,1)S(1)}, u32[]{:S(2)}, u32[]{:S(2)}) async-start(bf16[16,2,16384]{2,1,0:T(2,128)(2,1)} %reshape.378), calls=%async_computation.2 | async-start | bytes 2097152 | tf_op jit(solution)/shard_map/all_to_all | solution.py:150
  163.3 17.0 %all-to-all-done.2 = bf16[16,2,16384]{2,1,0:T(2,128)(2,1)S(1)} async-done(((bf16[16,2,16384]{2,1,0:T(2,128)(2,1)}), bf16[16,2,16384]{2,1,0:T(2,128)(2,1)S(1)}, u32[]{:S(2)}, u32[]{:S(2)}) %all-to-all-start.2) | async-done | bytes 1048608 | tf_op jit(solution)/shard_map/all_to_all | solution.py:150
  184.0 6.1 %multiply_reduce_fusion.1 = (f32[256]{0:T(256)S(1)}, f32[256,2048]{1,0:T(8,128)S(1)}) fusion(bf16[256,2048]{0,1:T(8,128)(2,1)S(1)} %bitcast.157, bf16[2048,2048]{1,0:T(8,128)(2,1)} %all-gather.5.cloned.1.call-done, bf16[1,256,2048]{2,1,0:T(8,128)(2,1)} %param.21), kind=kOutput, calls=%fused_computation.45 | convolution fusion | flops 2150629120 | bytes 12583936 | tf_op jit(solution)/shard_map/dot_general | solution.py:153
  190.3 6.0 %gather_fusion = bf16[1024,2048]{1,0:T(8,128)(2,1)} fusion(bf16[256,2048]{1,0:T(8,128)(2,1)S(1)} %multiply_convert_fusion.1, s32[1024]{0:T(1024)S(1)} %broadcast_clamp_fusion), kind=kCustom, calls=%fused_computation | custom fusion | bytes 8392704 | tf_op jit(solution)/shard_map/jit(_take)/gather | solution.py:64
  198.9 54.0 %all_to_all.55 = bf16[16,64,2048]{2,1,0:T(8,128)(2,1)S(1)} all-to-all(bf16[16,64,2048]{2,1,0:T(8,128)(2,1)S(1)} %select_select_fusion), channel_id=1, replica_groups=mesh['sp'=16,'dp'=8] {'sp'}, dimensions={0} | all-to-all | bytes 8388608 | tf_op jit(solution)/shard_map/all_to_all | solution.py:164
  253.0 4.5 %fusion.29 = f32[1024,1024]{1,0:T(8,128)S(1)} fusion(bf16[1024,2048]{1,0:T(8,128)(2,1)S(1)} %bitcast.160, bf16[1,2048,1024]{2,1,0:T(8,128)(2,1)S(1)} %copy-done.11), kind=kOutput, calls=%fused_computation.31 | convolution fusion | flops 4294967296 | bytes 12582912 | tf_op jit(solution)/shard_map/dot_general | solution.py:168
  257.5 5.4 %multiply_convert_fusion = bf16[1024,1024]{1,0:T(8,128)(2,1)S(1)} fusion(f32[1024,1024]{1,0:T(8,128)S(1)} %fusion.29, bf16[1024,2048]{1,0:T(8,128)(2,1)S(1)} %bitcast.161, bf16[1,2048,1024]{2,1,0:T(8,128)(2,1)S(1)} %copy-done.12), kind=kOutput, calls=%fused_computation.36 | convolution fusion | flops 4301258752 | bytes 14680064 | tf_op jit(solution)/shard_map/dot_general | solution.py:167
  262.8 6.1 %fusion.33 = bf16[1024,2048]{1,0:T(8,128)(2,1)} fusion(bf16[1024,1024]{1,0:T(8,128)(2,1)S(1)} %multiply_convert_fusion, bf16[1,1024,2048]{2,1,0:T(8,128)(2,1)S(1)} %copy-done.13), kind=kOutput, calls=%fused_computation.39 | convolution fusion | flops 4297064448 | bytes 10485760 | tf_op jit(solution)/shard_map/dot_general | solution.py:170
  268.9 4.9 %all-to-all-start.4 = ((bf16[16,64,2048]{2,1,0:T(8,128)(2,1)}), bf16[16,64,2048]{2,1,0:T(8,128)(2,1)}, u32[]{:S(2)}, u32[]{:S(2)}) async-start(bf16[16,64,2048]{2,1,0:T(8,128)(2,1)} %bitcast.159), calls=%async_computation.4 | async-start | bytes 8388608 | tf_op jit(solution)/shard_map/all_to_all | solution.py:173
  274.8 59.5 %all-to-all-done.4 = bf16[16,64,2048]{2,1,0:T(8,128)(2,1)} async-done(((bf16[16,64,2048]{2,1,0:T(8,128)(2,1)}), bf16[16,64,2048]{2,1,0:T(8,128)(2,1)}, u32[]{:S(2)}, u32[]{:S(2)}) %all-to-all-start.4) | async-done | bytes 4194336 | tf_op jit(solution)/shard_map/all_to_all | solution.py:173
  334.3 8.0 %gather_fusion.1 = bf16[512,2048]{1,0:T(8,128)(2,1)} fusion(bf16[1024,2048]{1,0:T(8,128)(2,1)} %bitcast.30, s32[1024]{0:T(1024)S(1)} %pad_clamp_fusion), kind=kCustom, calls=%fused_computation.1 | custom fusion | bytes 4196352 | tf_op jit(solution)/shard_map/jit(_take)/gather | solution.py:72
  342.3 4.4 %gather.15 = bf16[256,2,2048]{2,1,0:T(2,128)(2,1)} reshape(bf16[512,2048]{1,0:T(8,128)(2,1)} %gather_fusion.1) | data formatting | bytes 4194304 | tf_op jit(solution)/shard_map/jit(_take)/gather | solution.py:72
  346.7 9.9 %multiply_reduce_fusion = f32[256,2048]{1,0:T(8,128)S(1)} fusion(bf16[256,2,2048]{2,1,0:T(2,128)(2,1)} %gather.15, pred[256,2]{1,0:T(8,128)(4,1)S(1)} %copy.104, f32[256,2]{1,0:T(8,128)S(1)} %copy.99), kind=kLoop, calls=%fused_computation.35 | loop fusion | flops 3670016 | bytes 4196864 | tf_op jit(solution)/shard_map/reduce_sum | solution.py:74
  (150 shorter events, 89.2 us)
Async XLA Ops:
  6.5 60.0 %copy-start = (bf16[256,128]{1,0:T(8,128)(2,1)S(1)}, bf16[256,128]{1,0:T(8,128)(2,1)}, u32[]{:S(2)}) copy-start(bf16[256,128]{1,0:T(8,128)(2,1)} %param.23) | copy-start | bytes 196612
  6.5 14.5 %copy-start.4 = (bf16[1,256,16,128]{3,2,1,0:T(8,128)(2,1)S(1)}, bf16[1,256,16,128]{3,2,1,0:T(8,128)(2,1)}, u32[]{:S(2)}) copy-start(bf16[1,256,16,128]{3,2,1,0:T(8,128)(2,1)} %param.17) | copy-start | bytes 3145732
  6.5 58.6 %all-gather.3.cloned.1.call-start = ((), (), s32[]{:S(2)}) async-start(), calls=%async_computation.5 | async-start | bytes 3342336 | tf_op jit(solution)/shard_map/all_gather | solution.py:13
  11.9 26.1 %copy-start.5 = (bf16[128,256]{1,0:T(8,128)(2,1)S(1)}, bf16[128,256]{1,0:T(8,128)(2,1)}, u32[]{:S(2)}) copy-start(bf16[128,256]{1,0:T(8,128)(2,1)} %param.25) | copy-start | bytes 196612
  11.9 40.7 %copy-start.7 = (s32[1,256,2]{1,2,0:T(2,128)S(1)}, s32[1,256,2]{1,2,0:T(2,128)}, u32[]{:S(2)}) copy-start(s32[1,256,2]{1,2,0:T(2,128)} %param.30) | copy-start | bytes 6148
  12.9 21.4 %all-to-all-start.1 = ((bf16[256,16,64]{0,2,1:T(8,128)(2,1)}), bf16[256,16,64]{0,2,1:T(8,128)(2,1)S(1)}, u32[]{:S(2)}, u32[]{:S(2)}) async-start(bf16[256,16,64]{0,2,1:T(8,128)(2,1)} %pad_maximum_fusion), calls=%async_computation.1 | async-start | bytes 1048576 | tf_op jit(solution)/shard_map/all_to_all | solution.py:106
  34.3 36.3 %all-to-all-start = ((bf16[256,16,128]{2,0,1:T(8,128)(2,1)}), bf16[256,16,128]{2,0,1:T(8,128)(2,1)S(1)}, u32[]{:S(2)}, u32[]{:S(2)}) async-start(bf16[256,16,128]{2,0,1:T(8,128)(2,1)} %bitcast.139), calls=%async_computation | async-start | bytes 2097152 | tf_op jit(solution)/shard_map/all_to_all | solution.py:105
  38.0 146.0 %all-gather.5.cloned.1.call-start = ((), (), s32[]{:S(2)}) async-start(), calls=%async_computation.6 | async-start | bytes 8912896 | tf_op jit(solution)/shard_map/all_gather | solution.py:155
  54.6 14.3 %copy-start.6 = (bf16[256,128]{1,0:T(8,128)(2,1)S(1)}, bf16[256,128]{1,0:T(8,128)(2,1)}, u32[]{:S(2)}) copy-start(bf16[256,128]{1,0:T(8,128)(2,1)} %param.24) | copy-start | bytes 196612
  65.1 3.8 %copy-start.2 = (bf16[4096,320]{1,0:T(8,128)(2,1)S(1)}, bf16[4096,320]{1,0:T(8,128)(2,1)}, u32[]{:S(2)}) copy-start(bf16[4096,320]{1,0:T(8,128)(2,1)} %all-gather.3.cloned.1.call-done) | copy-start | bytes 7864324
  76.8 1.3 copy-start.3
  87.2 1.3 copy-start.3
  97.6 1.3 copy-start.3
  107.9 1.3 copy-start.3
  118.3 1.3 copy-start.3
  157.7 22.6 %all-to-all-start.2 = ((bf16[16,2,16384]{2,1,0:T(2,128)(2,1)}), bf16[16,2,16384]{2,1,0:T(2,128)(2,1)S(1)}, u32[]{:S(2)}, u32[]{:S(2)}) async-start(bf16[16,2,16384]{2,1,0:T(2,128)(2,1)} %reshape.378), calls=%async_computation.2 | async-start | bytes 2097152 | tf_op jit(solution)/shard_map/all_to_all | solution.py:150
  184.0 6.1 %copy-start.9 = (f32[2048]{0:T(1024)S(1)}, f32[2048]{0:T(1024)}, u32[]{:S(2)}) copy-start(f32[2048]{0:T(1024)} %param.26) | copy-start | bytes 24580
  198.9 54.0 %copy-start.11 = (bf16[1,2048,1024]{2,1,0:T(8,128)(2,1)S(1)}, bf16[1,2048,1024]{2,1,0:T(8,128)(2,1)}, u32[]{:S(2)}) copy-start(bf16[1,2048,1024]{2,1,0:T(8,128)(2,1)} %param.28) | copy-start | bytes 12582916
  253.0 4.5 %copy-start.12 = (bf16[1,2048,1024]{2,1,0:T(8,128)(2,1)S(1)}, bf16[1,2048,1024]{2,1,0:T(8,128)(2,1)}, u32[]{:S(2)}) copy-start(bf16[1,2048,1024]{2,1,0:T(8,128)(2,1)} %param.27) | copy-start | bytes 12582916
  257.5 5.4 %copy-start.13 = (bf16[1,1024,2048]{2,1,0:T(8,128)(2,1)S(1)}, bf16[1,1024,2048]{2,1,0:T(8,128)(2,1)}, u32[]{:S(2)}) copy-start(bf16[1,1024,2048]{2,1,0:T(8,128)(2,1)} %param.29) | copy-start | bytes 12582916
  268.9 5.0 %copy-start.8 = (s32[1,256,2]{1,2,0:T(2,128)S(1)}, s32[1,256,2]{1,2,0:T(2,128)}, u32[]{:S(2)}) copy-start(s32[1,256,2]{1,2,0:T(2,128)} %param.30) | copy-start | bytes 6148
  268.9 5.6 %copy-start.10 = (f32[1,256,2]{1,2,0:T(2,128)S(1)}, f32[1,256,2]{1,2,0:T(2,128)}, u32[]{:S(2)}) copy-start(f32[1,256,2]{1,2,0:T(2,128)} %param.31) | copy-start | bytes 6148
  268.9 65.4 %all-to-all-start.4 = ((bf16[16,64,2048]{2,1,0:T(8,128)(2,1)}), bf16[16,64,2048]{2,1,0:T(8,128)(2,1)}, u32[]{:S(2)}, u32[]{:S(2)}) async-start(bf16[16,64,2048]{2,1,0:T(8,128)(2,1)} %bitcast.159), calls=%async_computation.4 | async-start | bytes 8388608 | tf_op jit(solution)/shard_map/all_to_all | solution.py:173
  342.3 15.6 %copy-start.1 = (bf16[256,128]{1,0:T(8,128)(2,1)S(1)}, bf16[256,128]{1,0:T(8,128)(2,1)}, u32[]{:S(2)}) copy-start(bf16[256,128]{1,0:T(8,128)(2,1)} %param.23) | copy-start | bytes 196612
  (3 other events, 3.9 us)
Sparse Core Ops, SparseCore 0:
  10.8 54.2 all-gather.2
  67.2 70.0 all-gather.4
where the time goes:
time: 366 us; the launch traced here: 365 us
  waiting for transfers between devices  97.6 us (27%)
  matrix products  89 us (24%)
  blocking collectives  68.6 us (19%)
  other arithmetic  34.8 us (10%)
  local copies, waits for them, and re-layouts  34.5 us (9%)
  starting transfers between devices  21.6 us (6%)
  between operations  13.8 us (4%)
  loops' own time  4.87 us (1%)
    all_to_all x1, waiting for transfers between devices, shards(): lax.all_to_all(result.reshape(senders, slots_now, width), 'sp', split_axi...  59.5 us
    all_to_all x1, blocking collectives, shards(): lax.all_to_all(outgoing, 'sp', split_axis=0, concat_axis=0, tiled=True)  54 us
    dot_general x8, matrix products, one_block(): jnp.einsum('bhr,sr->hbs', turn_block, all_keyturn, preferred_element_type...  30 us
    dot_general x8, matrix products, one_block(): jnp.einsum('hbs,shd->bhd', attend, value_heads, preferred_element_type=jn...  22.9 us
    all_to_all x1, waiting for transfers between devices, shards(): lax.all_to_all(attended, 'sp', split_axis=0, concat_axis=1, tiled=True)  17 us
    all_gather x1, blocking collectives, shards(): head_rows = lax.all_gather(out_proj, 'dp', axis=1, tiled=True)  14.6 us
    gather x2, local copies, waits for them, and re-layouts, combine_slots(): jnp.take(flat_back, slot_ids, axis=0).astype(jnp.float32)  12.4 us
    all_to_all x1, waiting for transfers between devices, shards(): lax.all_to_all(query_turned, 'sp', split_axis=1, concat_axis=0, tiled=True)  12 us
  transfers between devices with their start and end apart: 6, of which 4 were waited for; matrix products, arithmetic and copies ran while one was open for 27% of the time, Pallas kernels for 0%

commit v1 on v0

--- a/solution.py
+++ b/solution.py
@@ -1,6 +1,8 @@
 import jax
 import jax.numpy as jnp
 from jax import lax
+from jax.experimental import pallas as pl
+from jax.experimental.pallas import tpu as pltpu
 from jax.sharding import PartitionSpec as P
 
 epsilon = 1e-06
@@ -44,34 +46,177 @@
     return floats * lax.rsqrt(jnp.mean(floats * floats, axis=-1, keepdims=True) + epsilon) * gain
 
 
-def assign_slots(route_block, experts_all, capacity):
-    flat_routes = route_block.reshape(-1)
-    onehot = (flat_routes[:, None] == jnp.arange(experts_all, dtype=jnp.int32)[None, :]).astype(
-        jnp.int32
-    )
-    earlier = jnp.cumsum(onehot, axis=0) - onehot
-    placed = jnp.sum(earlier * onehot, axis=1)
-    return flat_routes * capacity + placed
-
-
-def fill_slots(rows, slot_ids, experts_all, capacity):
-    pairs = slot_ids.shape[0]
-    matches = jnp.arange(experts_all * capacity, dtype=jnp.int32)[:, None] == slot_ids[None, :]
-    source = (
-        jnp.sum(jnp.where(matches, jnp.arange(pairs, dtype=jnp.int32)[None, :], 0), axis=1) // 2
-    )
-    filled = jnp.any(matches, axis=1)
-    picked = jnp.take(rows, source, axis=0)
-    chosen = jnp.where(filled[:, None], picked, jnp.zeros_like(picked))
-    return chosen.reshape(experts_all, capacity, rows.shape[-1])
-
-
-def combine_slots(returned, slot_ids, weights):
-    flat_back = returned.reshape(-1, returned.shape[-1])
-    picked = (
-        jnp.take(flat_back, slot_ids, axis=0).astype(jnp.float32).reshape(weights.shape[0], 2, -1)
-    )
-    return jnp.sum(weights[:, :, None] * picked, axis=1)
+ORDER = [(0, 0), (2, 2), (3, 2), (2, 3), (1, 2), (2, 1), (0, 2), (2, 0), (3, 1), (1, 3), (3, 3), (1, 1), (3, 0), (0, 3), (1, 0), (0, 1)]
+MESH = pl.DeviceIdType.MESH
+
+
+def shifted(me, dz, dy):
+    z, y = me // 4, lax.rem(me, 4)
+    return lax.rem(z + dz, 4) * 4 + lax.rem(y + dy, 4)
+
+
+def remote(src, dst, send, recv, target):
+    return pltpu.make_async_remote_copy(
+        src_ref=src,
+        dst_ref=dst,
+        send_sem=send,
+        recv_sem=recv,
+        device_id={"sp": target},
+        device_id_type=MESH,
+    )
+
+
+def experts_kernel(
+    heads, wo, resid, gain, routes, routes_t, weight, wg_hbm, wu_hbm, wd_hbm, out,
+    wg, wu, wd, after, normed, outgoing, arrived, hidden, result, returned, total,
+    wsem, send1, recv1, send2, recv2,
+):
+    me = lax.axis_index("sp")
+    f32, bf16, i32 = jnp.float32, jnp.bfloat16, jnp.int32
+    barrier = pltpu.get_barrier_semaphore()
+    for dz, dy in ORDER[1:]:
+        pl.semaphore_signal(barrier, inc=1, device_id={"sp": shifted(me, dz, dy)}, device_id_type=MESH)
+    loads = [
+        pltpu.make_async_copy(a, b, wsem.at[i])
+        for i, (a, b) in enumerate(((wg_hbm, wg), (wu_hbm, wu), (wd_hbm, wd)))
+    ]
+    for load in loads:
+        load.start()
+
+    @pl.loop(0, 8)
+    def _(n):
+        cols = pl.ds(pl.multiple_of(n * 256, 256), 256)
+        p = jnp.dot(heads[...], wo[:, cols], preferred_element_type=f32).astype(bf16)
+        after[:, cols] = resid[:, cols].astype(f32) + p.astype(f32)
+
+    @pl.loop(0, 8)
+    def _(r):
+        rows = pl.ds(pl.multiple_of(r * 32, 32), 32)
+        a = after[rows, :]
+        scale = lax.rsqrt(jnp.mean(a * a, axis=-1, keepdims=True) + epsilon)
+        normed[rows, :] = (a * scale * gain[...]).astype(bf16)
+
+    tok = lax.broadcasted_iota(i32, (256, 256), 0)
+    tok_l = lax.broadcasted_iota(i32, (256, 256), 1)
+    upper = jnp.where(tok < tok_l, 1.0, 0.0).astype(bf16)
+    lower = jnp.where(tok_l < tok, 1.0, 0.0).astype(bf16)
+    ex_t = lax.broadcasted_iota(i32, (16, 256), 0)
+    hot_t = [jnp.where(ex_t == routes_t[k : k + 1, :], 1.0, 0.0) for k in range(2)]
+    before_t = jnp.dot((hot_t[0] + hot_t[1]).astype(bf16), upper, preferred_element_type=f32)
+    base_t = before_t + (ex_t * 64).astype(f32)
+    slot_t = [jnp.sum(h * base_t, axis=0, keepdims=True).astype(i32) for h in hot_t]
+    ex_c = lax.broadcasted_iota(i32, (256, 128), 1)
+    hot_c = [jnp.where(ex_c == routes[:, k : k + 1], 1.0, 0.0) for k in range(2)]
+    before_c = jnp.dot(lower, (hot_c[0] + hot_c[1]).astype(bf16), preferred_element_type=f32)
+    base_c = before_c + (ex_c * 64).astype(f32)
+    slot_c = [jnp.sum(h * base_c, axis=1, keepdims=True).astype(i32) for h in hot_c]
+
+    def places(g, axis):
+        shape = (256, 1) if axis == 0 else (1, 256)
+        r = lax.broadcasted_iota(i32, shape, axis)
+        owner = [shifted(me, *ORDER[4 * g + j]) * 64 for j in range(4)]
+        base = jnp.where(r < 64, owner[0], jnp.where(r < 128, owner[1], jnp.where(r < 192, owner[2], owner[3])))
+        return base + (r & 63)
+
+    pl.semaphore_wait(barrier, 15)
+
+    first = [
+        None if k == 0 else remote(outgoing.at[k], arrived.at[k], send1.at[k], recv1.at[k], shifted(me, *ORDER[k]))
+        for k in range(16)
+    ]
+    for g in range(4):
+        place = places(g, 0)
+        pick = jnp.where((slot_t[0] == place) | (slot_t[1] == place), 1.0, 0.0).astype(bf16)
+        for n in range(4):
+            cols = slice(n * 512, n * 512 + 512)
+            rows = jnp.dot(pick, normed[:, cols], preferred_element_type=f32).astype(bf16)
+            for j in range(4):
+                k = 4 * g + j
+                (arrived if k == 0 else outgoing)[k, :, cols] = rows[j * 64 : j * 64 + 64]
+        if g > 0:
+            for k in range(max(1, 4 * g - 4), 4 * g):
+                first[k].start()
+    for load in loads:
+        load.wait()
+    for k in range(12, 16):
+        first[k].start()
+
+    second = [
+        None if k == 0 else remote(result.at[k], returned.at[k], send2.at[k], recv2.at[k], shifted(me, (4 - ORDER[k][0]) % 4, (4 - ORDER[k][1]) % 4))
+        for k in range(16)
+    ]
+    for g in range(4):
+        for k in range(max(1, 4 * g), 4 * g + 4):
+            first[k].wait_recv()
+
+        @pl.loop(0, 4)
+        def _(n):
+            cols = pl.ds(pl.multiple_of(n * 256, 256), 256)
+            rows = arrived[4 * g : 4 * g + 4].reshape(256, 2048)
+            gate = jnp.dot(rows, wg[:, cols], preferred_element_type=f32)
+            up = jnp.dot(rows, wu[:, cols], preferred_element_type=f32)
+            hidden[:, cols] = (gate / (1.0 + jnp.exp(-gate)) * up).astype(bf16)
+
+        @pl.loop(0, 4)
+        def _(n):
+            cols = pl.ds(pl.multiple_of(n * 512, 512), 512)
+            rows = jnp.dot(hidden[...], wd[:, cols], preferred_element_type=f32).astype(bf16)
+            for j in range(4):
+                k = 4 * g + j
+                (returned if k == 0 else result)[k, :, cols] = rows[j * 64 : j * 64 + 64]
+
+        for k in range(max(1, 4 * g), 4 * g + 4):
+            second[k].start()
+
+    for g in range(4):
+        place = places(g, 1)
+        picks = [jnp.where(s == place, 1.0, 0.0).astype(bf16) for s in slot_c]
+        for k in range(max(1, 4 * g), 4 * g + 4):
+            second[k].wait_recv()
+        for n in range(4):
+            cols = slice(n * 512, n * 512 + 512)
+            rows = returned[4 * g : 4 * g + 4, :, cols].reshape(256, 512)
+            t = weight[:, 0:1] * jnp.dot(picks[0], rows, preferred_element_type=f32)
+            t = t + weight[:, 1:2] * jnp.dot(picks[1], rows, preferred_element_type=f32)
+            if g > 0:
+                t = t + total[:, cols]
+            if g < 3:
+                total[:, cols] = t
+            else:
+                out[:, cols] = (after[:, cols] + t).astype(bf16)
+    for k in range(1, 16):
+        first[k].wait_send()
+        second[k].wait_send()
+
+
+def experts(heads, wo, resid, gain, routes, weight, wg, wu, wd):
+    v, a = pl.BlockSpec(memory_space=pltpu.VMEM), pl.BlockSpec(memory_space=pl.ANY)
+    bf16, f32 = jnp.bfloat16, jnp.float32
+    return pl.pallas_call(
+        experts_kernel,
+        name="experts",
+        out_shape=jax.ShapeDtypeStruct((256, 2048), bf16),
+        in_specs=[v] * 7 + [a] * 3,
+        out_specs=v,
+        scratch_shapes=[
+            pltpu.VMEM((2048, 1024), bf16),
+            pltpu.VMEM((2048, 1024), bf16),
+            pltpu.VMEM((1024, 2048), bf16),
+            pltpu.VMEM((256, 2048), f32),
+            pltpu.VMEM((256, 2048), bf16),
+            pltpu.VMEM((16, 64, 2048), bf16),
+            pltpu.VMEM((16, 64, 2048), bf16),
+            pltpu.VMEM((256, 1024), bf16),
+            pltpu.VMEM((16, 64, 2048), bf16),
+            pltpu.VMEM((16, 64, 2048), bf16),
+            pltpu.VMEM((256, 2048), f32),
+            pltpu.SemaphoreType.DMA((3,)),
+        ]
+        + [pltpu.SemaphoreType.DMA((16,))] * 4,
+        compiler_params=pltpu.CompilerParams(
+            collective_id=1, has_side_effects=True, vmem_limit_bytes=60 * 1024 * 1024
+        ),
+    )(heads, wo, resid, gain, routes, routes.T, weight, wg, wu, wd)
 
 
 def shards(
@@ -150,31 +295,11 @@
     token_heads = lax.all_to_all(attended, "sp", split_axis=0, concat_axis=1, tiled=True)
     flat_heads = token_heads.reshape(tokens_here, -1)
     head_rows = lax.all_gather(out_proj, "dp", axis=1, tiled=True)
-    projected = jnp.dot(
-        flat_heads,
-        lax.all_gather(head_rows, "sp", axis=0, tiled=True),
-        preferred_element_type=jnp.float32,
-    ).astype(jnp.bfloat16)
-    after_attention = resid[0].astype(jnp.float32) + projected.astype(jnp.float32)
-    normed = rms_scaled(after_attention, norm_gain).astype(jnp.bfloat16)
-    experts_all = sp_count * expert_gate.shape[0]
-    capacity = 4 * tokens_here // experts_all
-    slot_ids = assign_slots(routes[0], experts_all, capacity)
-    outgoing = fill_slots(normed, slot_ids, experts_all, capacity)
-    arrived = lax.all_to_all(outgoing, "sp", split_axis=0, concat_axis=0, tiled=True)
-    senders, slots_now, width = arrived.shape
-    rows = arrived.reshape(senders * slots_now, width)
-    gate = jnp.dot(rows, expert_gate[0], preferred_element_type=jnp.float32)
-    upward = jnp.dot(rows, expert_up[0], preferred_element_type=jnp.float32)
-    hidden = (jax.nn.silu(gate) * upward).astype(jnp.bfloat16)
-    result = jnp.dot(hidden, expert_down[0], preferred_element_type=jnp.float32).astype(
-        jnp.bfloat16
-    )
-    returned = lax.all_to_all(
-        result.reshape(senders, slots_now, width), "sp", split_axis=0, concat_axis=0, tiled=True
-    )
-    routed = combine_slots(returned, slot_ids, route_weight[0])
-    return (after_attention + routed).astype(jnp.bfloat16)[None]
+    wo = lax.all_gather(head_rows, "sp", axis=0, tiled=True)
+    return experts(
+        flat_heads, wo, resid[0], norm_gain[None], routes[0], route_weight[0],
+        expert_gate[0], expert_up[0], expert_down[0],
+    )[None]
 
 
 def solution(mesh):

time: 366 us -> 323 us (0.88)
  the two profiles are of different devices: /device:TPU:0 before, /device:TPU:20 now
where the time goes in v1:
time: 323 us; the launch traced here: 322 us
  Pallas kernels  131 us (41%)
  matrix products  68.6 us (21%)
  waiting for transfers between devices  32 us (10%)
  starting transfers between devices  21.2 us (7%)
  other arithmetic  18.9 us (6%)
  local copies, waits for them, and re-layouts  17.9 us (6%)
  between operations  13.6 us (4%)
  blocking collectives  13 us (4%)
  loops' own time  5.4 us (2%)
    pallas_call x1, Pallas kernels, experts(): pl.pallas_call(experts_kernel, name='experts', out_shape=jax.ShapeDtypeSt...  131 us
    dot_general x8, matrix products, one_block(): jnp.einsum('bhr,sr->hbs', turn_block, all_keyturn, preferred_element_type...  30 us
    dot_general x8, matrix products, one_block(): jnp.einsum('hbs,shd->bhd', attend, value_heads, preferred_element_type=jn...  22.9 us
    all_to_all x1, waiting for transfers between devices, shards(): lax.all_to_all(attended, 'sp', split_axis=0, concat_axis=1, tiled=True)  13 us
    all_gather x1, blocking collectives, shards(): head_rows = lax.all_gather(out_proj, 'dp', axis=1, tiled=True)  13 us
    all_gather x1, waiting for transfers between devices, sent_together(): lax.all_gather(both, axis, axis=dim, tiled=True)  11.4 us
    reduce_sum x8, other arithmetic, one_block(): jnp.sum(powers, axis=-1, keepdims=True)  10.2 us
    unnamed x18, local copies, waits for them, and re-layouts  10.2 us
  transfers between devices with their start and end apart: 5, of which 3 were waited for; matrix products, arithmetic and copies ran while one was open for 31% of the time, Pallas kernels for 0%

profile of v1, /device:TPU:20, one launch (start us, length us, event | category | flops | bytes accessed | tf_op | source)
XLA Modules:
  0.0 321.5 jit_solution(1808075168659293132)
XLA Ops:
  12.8 8.3 %all-to-all-start.1 = ((bf16[256,16,64]{0,2,1:T(8,128)(2,1)}), bf16[256,16,64]{0,2,1:T(8,128)(2,1)S(1)}, u32[]{:S(2)}, u32[]{:S(2)}) async-start(bf16[256,16,64]{0,2,1:T(8,128)(2,1)} %pad_maximum_fusion), calls=%async_computation.1 | async-start | bytes 1048576 | tf_op jit(solution)/shard_map/all_to_all | solution.py:251
  23.7 7.5 %all-to-all-done.1 = bf16[256,16,64]{0,2,1:T(8,128)(2,1)S(1)} async-done(((bf16[256,16,64]{0,2,1:T(8,128)(2,1)}), bf16[256,16,64]{0,2,1:T(8,128)(2,1)S(1)}, u32[]{:S(2)}, u32[]{:S(2)}) %all-to-all-start.1) | async-done | bytes 524320 | tf_op jit(solution)/shard_map/all_to_all | solution.py:251
  31.2 6.7 %all-to-all-start = ((bf16[256,16,128]{2,0,1:T(8,128)(2,1)}), bf16[256,16,128]{2,0,1:T(8,128)(2,1)S(1)}, u32[]{:S(2)}, u32[]{:S(2)}) async-start(bf16[256,16,128]{2,0,1:T(8,128)(2,1)} %bitcast.99), calls=%async_computation | async-start | bytes 2097152 | tf_op jit(solution)/shard_map/all_to_all | solution.py:250
  38.0 13.0 %all_gather.10 = bf16[128,2048]{1,0:T(8,128)(2,1)} all-gather(bf16[128,256]{1,0:T(8,128)(2,1)S(1)} %copy-done.2), channel_id=1, replica_groups=mesh['sp'=16,'dp'=8] {'dp'}, dimensions={1}, use_global_device_ids=true | all-gather | bytes 589824 | tf_op jit(solution)/shard_map/all_gather | solution.py:297
  52.4 11.4 %all-gather.3.cloned.1.call-done = bf16[4096,320]{1,0:T(8,128)(2,1)} async-done(((bf16[256,320]{1,0:T(8,128)(2,1)}), bf16[4096,320]{1,0:T(8,128)(2,1)}) %all-gather.3.cloned.1.call-update) | async-done | bytes 2621456 | tf_op jit(solution)/shard_map/all_gather | solution.py:15
  66.2 3.3 %fusion.26 = bf16[4096,1,128]{2,0,1:T(8,128)(2,1)} fusion(bf16[256,128]{1,0:T(8,128)(2,1)S(1)} %copy-done.3, bf16[4096,320]{1,0:T(8,128)(2,1)} %all-gather.3.cloned.1.call-done), kind=kOutput, calls=%fused_computation.26 | convolution fusion | flops 268959744 | bytes 3211264 | tf_op jit(solution)/shard_map/dot_general | solution.py:260
  69.6 83.5 %while.11 = (s32[]{:T(128)}, bf16[8,512,1,128]{3,1,2,0:T(8,128)(2,1)}, s32[8]{0:T(128)S(1)}, bf16[8,512,1,128]{3,1,2,0:T(8,128)(2,1)S(1)}, bf16[4096,1,128]{2,0,...) while((s32[]{:T(128)}, ...), condition=%wide.region_4.5_spmd.clone, body=%wide.region_1.4_spmd.clone.sunk | while | flops 1363213824 | bytes 49101984 | solution.py:286
  72.1 3.7 %fusion.51 = (f32[512]{0:T(512)S(1)}, f32[1,512,4096]{2,1,0:T(8,128)S(1)}) fusion(bf16[4096,64]{1,0:T(8,128)(2,1)S(1)} %get-tuple-element.216, bf16[8,512,1,64]{1,3,2,0:T(8,128)(2,1)} %get-tuple-element.215, s32[]{:T(128)} %get-tuple-element.200, f32[512,4096]{1,0:T(8,128)S(1)} %fusion.50, s32[512]{0:T(512)S(1)} %iota_add_fusion.2), kind=kOutput, calls=%fused_computation.49.clone.1 | convolution fusion | flops 278920704 | bytes 17371648 | tf_op jit(solution)/shard_map/while/body/eval_jaxpr/bhr,sr->hbs/dot_general | solution.py:274
  77.2 2.9 fusion.53
  82.6 3.7 %fusion.51 = (f32[512]{0:T(512)S(1)}, f32[1,512,4096]{2,1,0:T(8,128)S(1)}) fusion(bf16[4096,64]{1,0:T(8,128)(2,1)S(1)} %get-tuple-element.216, bf16[8,512,1,64]{1,3,2,0:T(8,128)(2,1)} %get-tuple-element.215, s32[]{:T(128)} %get-tuple-element.200, f32[512,4096]{1,0:T(8,128)S(1)} %fusion.50, s32[512]{0:T(512)S(1)} %iota_add_fusion.2), kind=kOutput, calls=%fused_computation.49.clone.1 | convolution fusion | flops 278920704 | bytes 17371648 | tf_op jit(solution)/shard_map/while/body/eval_jaxpr/bhr,sr->hbs/dot_general | solution.py:274
  93.0 3.8 %fusion.51 = (f32[512]{0:T(512)S(1)}, f32[1,512,4096]{2,1,0:T(8,128)S(1)}) fusion(bf16[4096,64]{1,0:T(8,128)(2,1)S(1)} %get-tuple-element.216, bf16[8,512,1,64]{1,3,2,0:T(8,128)(2,1)} %get-tuple-element.215, s32[]{:T(128)} %get-tuple-element.200, f32[512,4096]{1,0:T(8,128)S(1)} %fusion.50, s32[512]{0:T(512)S(1)} %iota_add_fusion.2), kind=kOutput, calls=%fused_computation.49.clone.1 | convolution fusion | flops 278920704 | bytes 17371648 | tf_op jit(solution)/shard_map/while/body/eval_jaxpr/bhr,sr->hbs/dot_general | solution.py:274
  98.0 2.9 fusion.53
  103.4 3.7 %fusion.51 = (f32[512]{0:T(512)S(1)}, f32[1,512,4096]{2,1,0:T(8,128)S(1)}) fusion(bf16[4096,64]{1,0:T(8,128)(2,1)S(1)} %get-tuple-element.216, bf16[8,512,1,64]{1,3,2,0:T(8,128)(2,1)} %get-tuple-element.215, s32[]{:T(128)} %get-tuple-element.200, f32[512,4096]{1,0:T(8,128)S(1)} %fusion.50, s32[512]{0:T(512)S(1)} %iota_add_fusion.2), kind=kOutput, calls=%fused_computation.49.clone.1 | convolution fusion | flops 278920704 | bytes 17371648 | tf_op jit(solution)/shard_map/while/body/eval_jaxpr/bhr,sr->hbs/dot_general | solution.py:274
  108.5 2.9 fusion.53
  113.8 3.8 %fusion.51 = (f32[512]{0:T(512)S(1)}, f32[1,512,4096]{2,1,0:T(8,128)S(1)}) fusion(bf16[4096,64]{1,0:T(8,128)(2,1)S(1)} %get-tuple-element.216, bf16[8,512,1,64]{1,3,2,0:T(8,128)(2,1)} %get-tuple-element.215, s32[]{:T(128)} %get-tuple-element.200, f32[512,4096]{1,0:T(8,128)S(1)} %fusion.50, s32[512]{0:T(512)S(1)} %iota_add_fusion.2), kind=kOutput, calls=%fused_computation.49.clone.1 | convolution fusion | flops 278920704 | bytes 17371648 | tf_op jit(solution)/shard_map/while/body/eval_jaxpr/bhr,sr->hbs/dot_general | solution.py:274
  118.9 2.9 fusion.53
  124.3 3.8 %fusion.51 = (f32[512]{0:T(512)S(1)}, f32[1,512,4096]{2,1,0:T(8,128)S(1)}) fusion(bf16[4096,64]{1,0:T(8,128)(2,1)S(1)} %get-tuple-element.216, bf16[8,512,1,64]{1,3,2,0:T(8,128)(2,1)} %get-tuple-element.215, s32[]{:T(128)} %get-tuple-element.200, f32[512,4096]{1,0:T(8,128)S(1)} %fusion.50, s32[512]{0:T(512)S(1)} %iota_add_fusion.2), kind=kOutput, calls=%fused_computation.49.clone.1 | convolution fusion | flops 278920704 | bytes 17371648 | tf_op jit(solution)/shard_map/while/body/eval_jaxpr/bhr,sr->hbs/dot_general | solution.py:274
  129.4 2.9 fusion.53
  134.7 3.8 %fusion.51 = (f32[512]{0:T(512)S(1)}, f32[1,512,4096]{2,1,0:T(8,128)S(1)}) fusion(bf16[4096,64]{1,0:T(8,128)(2,1)S(1)} %get-tuple-element.216, bf16[8,512,1,64]{1,3,2,0:T(8,128)(2,1)} %get-tuple-element.215, s32[]{:T(128)} %get-tuple-element.200, f32[512,4096]{1,0:T(8,128)S(1)} %fusion.50, s32[512]{0:T(512)S(1)} %iota_add_fusion.2), kind=kOutput, calls=%fused_computation.49.clone.1 | convolution fusion | flops 278920704 | bytes 17371648 | tf_op jit(solution)/shard_map/while/body/eval_jaxpr/bhr,sr->hbs/dot_general | solution.py:274
  139.8 2.9 fusion.53
  145.2 3.7 %fusion.51 = (f32[512]{0:T(512)S(1)}, f32[1,512,4096]{2,1,0:T(8,128)S(1)}) fusion(bf16[4096,64]{1,0:T(8,128)(2,1)S(1)} %get-tuple-element.216, bf16[8,512,1,64]{1,3,2,0:T(8,128)(2,1)} %get-tuple-element.215, s32[]{:T(128)} %get-tuple-element.200, f32[512,4096]{1,0:T(8,128)S(1)} %fusion.50, s32[512]{0:T(512)S(1)} %iota_add_fusion.2), kind=kOutput, calls=%fused_computation.49.clone.1 | convolution fusion | flops 278920704 | bytes 17371648 | tf_op jit(solution)/shard_map/while/body/eval_jaxpr/bhr,sr->hbs/dot_general | solution.py:274
  157.5 6.2 %all-to-all-start.2 = ((bf16[16,2,16384]{2,1,0:T(2,128)(2,1)}), bf16[16,2,16384]{2,1,0:T(2,128)(2,1)S(1)}, u32[]{:S(2)}, u32[]{:S(2)}) async-start(bf16[16,2,16384]{2,1,0:T(2,128)(2,1)} %reshape.189), calls=%async_computation.2 | async-start | bytes 2097152 | tf_op jit(solution)/shard_map/all_to_all | solution.py:295
  165.3 13.0 %all-to-all-done.2 = bf16[16,2,16384]{2,1,0:T(2,128)(2,1)S(1)} async-done(((bf16[16,2,16384]{2,1,0:T(2,128)(2,1)}), bf16[16,2,16384]{2,1,0:T(2,128)(2,1)S(1)}, u32[]{:S(2)}, u32[]{:S(2)}) %all-to-all-start.2) | async-done | bytes 1048608 | tf_op jit(solution)/shard_map/all_to_all | solution.py:295
  181.4 131.0 %experts.1 = bf16[256,2048]{1,0:T(8,128)(2,1)} custom-call(bf16[256,2048]{1,0:T(8,128)(2,1)} %bitcast.116, bf16[2048,2048]{1,0:T(8,128)(2,1)} %all-gather.5.cloned.1.call-done.wo, bf16[256,2048]{1,0:T(8,128)(2,1)} %bitcast.125, f32[1,2048]{1,0:T(1,128)} %bitcast.127, s32[256,2]{1,0:T(8,128)} %copy.65.routes, s32[2,256]{1,0:T(2,128)} %bitcast.128, ...), custom_call_target="tpu_custom_call" | custom-call | tf_op jit(solution)/shard_map/experts/pallas_call | solution.py:195
  (98 shorter events, 55.0 us)
Async XLA Ops:
  6.5 57.3 %copy-start = (bf16[256,128]{1,0:T(8,128)(2,1)S(1)}, bf16[256,128]{1,0:T(8,128)(2,1)}, u32[]{:S(2)}) copy-start(bf16[256,128]{1,0:T(8,128)(2,1)} %param.23) | copy-start | bytes 196612
  6.5 31.4 %copy-start.2 = (bf16[128,256]{1,0:T(8,128)(2,1)S(1)}, bf16[128,256]{1,0:T(8,128)(2,1)}, u32[]{:S(2)}) copy-start(bf16[128,256]{1,0:T(8,128)(2,1)} %param.25) | copy-start | bytes 196612
  6.5 57.3 %all-gather.3.cloned.1.call-start = ((), (), s32[]{:S(2)}) async-start(), calls=%async_computation.3 | async-start | bytes 3342336 | tf_op jit(solution)/shard_map/all_gather | solution.py:15
  11.8 54.4 %copy-start.3 = (bf16[256,128]{1,0:T(8,128)(2,1)S(1)}, bf16[256,128]{1,0:T(8,128)(2,1)}, u32[]{:S(2)}) copy-start(bf16[256,128]{1,0:T(8,128)(2,1)} %param.24) | copy-start | bytes 196612
  12.8 18.4 %all-to-all-start.1 = ((bf16[256,16,64]{0,2,1:T(8,128)(2,1)}), bf16[256,16,64]{0,2,1:T(8,128)(2,1)S(1)}, u32[]{:S(2)}, u32[]{:S(2)}) async-start(bf16[256,16,64]{0,2,1:T(8,128)(2,1)} %pad_maximum_fusion), calls=%async_computation.1 | async-start | bytes 1048576 | tf_op jit(solution)/shard_map/all_to_all | solution.py:251
  31.2 38.3 %all-to-all-start = ((bf16[256,16,128]{2,0,1:T(8,128)(2,1)}), bf16[256,16,128]{2,0,1:T(8,128)(2,1)S(1)}, u32[]{:S(2)}, u32[]{:S(2)}) async-start(bf16[256,16,128]{2,0,1:T(8,128)(2,1)} %bitcast.99), calls=%async_computation | async-start | bytes 2097152 | tf_op jit(solution)/shard_map/all_to_all | solution.py:250
  37.9 143.5 %all-gather.5.cloned.1.call-start = ((), (), s32[]{:S(2)}) async-start(), calls=%async_computation.4 | async-start | bytes 8912896 | tf_op jit(solution)/shard_map/all_gather | solution.py:298
  63.8 5.7 %slice-start = ((bf16[4096,320]{1,0:T(8,128)(2,1)}), bf16[4096,64]{1,0:T(8,128)(2,1)S(1)}, s32[]{:S(2)}) async-start(bf16[4096,320]{1,0:T(8,128)(2,1)} %all-gather.3.cloned.1.call-done), calls=%async_computation.5 | async-start | bytes 2097152 | tf_op jit(solution)/shard_map/slice | solution.py:17
  69.5 94.1 %copy-start.5 = (f32[1,256,2]{1,2,0:T(2,128)S(1)}, f32[1,256,2]{1,2,0:T(2,128)}, u32[]{:S(2)}) copy-start(f32[1,256,2]{1,2,0:T(2,128)} %param.31) | copy-start | bytes 6148
  69.6 94.9 %copy-start.4 = (s32[1,256,2]{1,2,0:T(2,128)S(1)}, s32[1,256,2]{1,2,0:T(2,128)}, u32[]{:S(2)}) copy-start(s32[1,256,2]{1,2,0:T(2,128)} %param.30) | copy-start | bytes 6148
  75.9 1.3 copy-start.1
  86.3 1.3 copy-start.1
  96.7 1.3 copy-start.1
  107.2 1.3 copy-start.1
  117.6 1.3 copy-start.1
  128.1 1.3 copy-start.1
  138.5 1.3 copy-start.1
  148.9 1.3 copy-start.1
  157.5 20.8 %all-to-all-start.2 = ((bf16[16,2,16384]{2,1,0:T(2,128)(2,1)}), bf16[16,2,16384]{2,1,0:T(2,128)(2,1)S(1)}, u32[]{:S(2)}, u32[]{:S(2)}) async-start(bf16[16,2,16384]{2,1,0:T(2,128)(2,1)} %reshape.189), calls=%async_computation.2 | async-start | bytes 2097152 | tf_op jit(solution)/shard_map/all_to_all | solution.py:295
Sparse Core Ops, SparseCore 0:
  10.8 52.9 all-gather.2
  66.0 70.9 all-gather.4

commit v2 on v1

--- a/solution.py
+++ b/solution.py
@@ -8,15 +8,6 @@
 epsilon = 1e-06
 rope_base = 10000.0
 masked_score = -1e30
-
-
-def sent_together(arrays, axis, dim, along):
-    both = jnp.concatenate(arrays, axis=along)
-    out, at, finished = (lax.all_gather(both, axis, axis=dim, tiled=True), 0, [])
-    for a in arrays:
-        finished.append(lax.slice_in_dim(out, at, at + a.shape[along], axis=along))
-        at += a.shape[along]
-    return tuple(finished)
 
 
 def rotate(values, positions):
@@ -50,6 +41,14 @@
 MESH = pl.DeviceIdType.MESH
 
 
+def packed(digits):
+    value = sum(d << (2 * i) for i, d in enumerate(digits))
+    return value - (1 << 32) if value >= 1 << 31 else value
+
+
+ZS, YS = packed([o[0] for o in ORDER]), packed([o[1] for o in ORDER])
+
+
 def shifted(me, dz, dy):
     z, y = me // 4, lax.rem(me, 4)
     return lax.rem(z + dz, 4) * 4 + lax.rem(y + dy, 4)
@@ -66,27 +65,203 @@
     )
 
 
-def experts_kernel(
-    heads, wo, resid, gain, routes, routes_t, weight, wg_hbm, wu_hbm, wd_hbm, out,
+def layer_kernel(
+    q_in_hbm, lat_a, lat_b, up_kv, wo_hbm, resid, gain, routes, routes_t, weight, wg_hbm, wu_hbm, wd_hbm, out,
     wg, wu, wd, after, normed, outgoing, arrived, hidden, result, returned, total,
+    q_in, la, lb, keys, vals, q_cat, attended, heads, wo,
     wsem, send1, recv1, send2, recv2,
+    lsem, sa1, ra1, sb1, rb1, sa2, ra2, sb2, rb2, sq, rq, so, ro, swz, rwz, swy, rwy, swx, rwx, swc, rwc,
 ):
-    me = lax.axis_index("sp")
+    me, dp = lax.axis_index("sp"), lax.axis_index("dp")
+    z, y = me // 4, lax.rem(me, 4)
+    x, core = dp // 2, lax.rem(dp, 2)
     f32, bf16, i32 = jnp.float32, jnp.bfloat16, jnp.int32
     barrier = pltpu.get_barrier_semaphore()
     for dz, dy in ORDER[1:]:
         pl.semaphore_signal(barrier, inc=1, device_id={"sp": shifted(me, dz, dy)}, device_id_type=MESH)
+    x_peer = [None] + [lax.rem(x + d, 4) * 2 + core for d in (1, 2, 3)]
+    x_from = [dp] + [lax.rem(x + 4 - d, 4) * 2 + core for d in (1, 2, 3)]
+    other = x * 2 + 1 - core
+    for t in x_peer[1:] + [other]:
+        pl.semaphore_signal(barrier, inc=1, device_id={"dp": t}, device_id_type=MESH)
+    fill_wo = pltpu.make_async_copy(wo_hbm, wo.at[dp, z, y], lsem.at[0])
+    fill_wo.start()
+    fill_q = pltpu.make_async_copy(q_in_hbm.at[me], q_in.at[0], lsem.at[1])
+    fill_q.start()
+    fill_a = pltpu.make_async_copy(lat_a, la.at[z, y], lsem.at[2])
+    fill_a.start()
+    fill_b = pltpu.make_async_copy(lat_b, lb.at[z, y], lsem.at[3])
+    fill_b.start()
     loads = [
         pltpu.make_async_copy(a, b, wsem.at[i])
         for i, (a, b) in enumerate(((wg_hbm, wg), (wu_hbm, wu), (wd_hbm, wd)))
     ]
     for load in loads:
         load.start()
+    fill_a.wait()
+    fill_b.wait()
+    fill_wo.wait()
+    pl.semaphore_wait(barrier, 19)
+
+    def along(dz, dy):
+        return shifted(me, dz, dy)
+
+    a1 = [remote(la.at[z, y], la.at[z, y], sa1.at[d], ra1.at[d], along(d, 0)) for d in (1, 2, 3)]
+    b1 = [remote(lb.at[z, y], lb.at[z, y], sb1.at[d], rb1.at[d], along(0, d)) for d in (1, 2, 3)]
+    w1 = [remote(wo.at[dp, z, y], wo.at[dp, z, y], swz.at[d], rwz.at[d], along(d, 0)) for d in (1, 2, 3)]
+    a2 = [remote(la.at[:, y], la.at[:, y], sa2.at[d], ra2.at[d], along(0, d)) for d in (1, 2, 3)]
+    b2 = [remote(lb.at[z], lb.at[z], sb2.at[d], rb2.at[d], along(d, 0)) for d in (1, 2, 3)]
+    w2 = [remote(wo.at[dp, :, y], wo.at[dp, :, y], swy.at[d], rwy.at[d], along(0, d)) for d in (1, 2, 3)]
+    asks = [
+        None if k == 0 else remote(q_in_hbm.at[along(*ORDER[k])], q_in.at[k], sq.at[k], rq.at[k], along(*ORDER[k]))
+        for k in range(16)
+    ]
+
+    def to_x(g):
+        part = wo.at[dp, :, lax.rem(y + 4 - g, 4)]
+        copies = [
+            pltpu.make_async_remote_copy(
+                src_ref=part, dst_ref=part, send_sem=swx.at[g, d], recv_sem=rwx.at[g, d],
+                device_id={"dp": x_peer[d]}, device_id_type=MESH,
+            )
+            for d in (1, 2, 3)
+        ]
+        return copies
+
+    def to_core(g, d):
+        part = wo.at[x_from[d], :, lax.rem(y + 4 - g, 4)]
+        return pltpu.make_async_remote_copy(
+            src_ref=part, dst_ref=part, send_sem=swc.at[g, d], recv_sem=rwc.at[g, d],
+            device_id={"dp": other}, device_id_type=MESH,
+        )
+
+    for c in a1 + b1 + w1:
+        c.start()
+    for c in a1:
+        c.wait_recv()
+    for c in a2:
+        c.start()
+    for c in b1:
+        c.wait_recv()
+    for c in b2:
+        c.start()
+    for c in w1:
+        c.wait_recv()
+    for c in w2 + to_x(0) + [to_core(0, 0)]:
+        c.start()
+    for c in asks[1:]:
+        c.start()
+
+    vals[:, 128:256] = jnp.ones((4096, 128), bf16)
+    for c in a2 + b2:
+        c.wait_recv()
+
+    @pl.loop(0, 16)
+    def _(b):
+        bz, by = b // 4, lax.rem(b, 4)
+        rows = pl.ds(pl.multiple_of(b * 256, 256), 256)
+        lat = jnp.concatenate([la[bz, by], lb[bz, by, 0:256, :]], axis=1)
+        kv = jnp.dot(lat, up_kv[...], preferred_element_type=f32).astype(bf16)
+        keys[rows, 0:128] = kv[:, 0:128]
+        vals[rows, 0:128] = kv[:, 128:256]
+        turn = lb[bz, by, 256:384, :].astype(f32)
+        swap = pltpu.roll(turn, 64, 1)
+        low = lax.broadcasted_iota(i32, (128, 128), 1) < 64
+        start = pl.multiple_of(b * 256, 256)
+        keys[pl.ds(start, 128), 128:256] = jnp.where(low, turn, swap).astype(bf16)
+        keys[pl.ds(pl.multiple_of(start + 128, 128), 128), 128:256] = jnp.where(low, swap, turn).astype(bf16)
+
+    fill_q.wait()
+    unit = 192.0 ** -0.5
+
+    def one_block(k, _):
+        dz, dy = (ZS >> (2 * k)) & 3, (YS >> (2 * k)) & 3
+        source = shifted(me, 4 - dz, 4 - dy)
+
+        @pl.when(k > 0)
+        def _():
+            remote(q_in.at[k], q_in.at[k], sq.at[k], rq.at[k], source).wait_recv()
+
+        for g in (1, 2, 3):
+
+            @pl.when(k == 4 * g - 2)
+            def _(g=g):
+                w2[g - 1].wait_recv()
+                for c in to_x(g) + [to_core(g, 0)]:
+                    c.start()
+
+        for g in (0, 1, 2):
+
+            @pl.when(k == 5 * g + 5)
+            def _(g=g):
+                for d in (1, 2, 3):
+                    to_x(g)[d - 1].wait_recv()
+                    to_core(g, d).start()
+
+        q_cat[:, 0:128] = q_in[k, 0:256, :]
+        turn = q_in[k, 256:384, :]
+        low = lax.broadcasted_iota(i32, (128, 128), 1) < 64
+        zero = jnp.zeros((128, 128), bf16)
+        q_cat[0:128, 128:256] = jnp.where(low, turn, zero)
+        q_cat[128:256, 128:256] = jnp.where(low, zero, turn)
+        q = q_cat[...]
+
+        def scores(at):
+            return lax.dot_general(
+                q, keys[pl.ds(at, 512), :], (((1,), (1,)), ((), ())), preferred_element_type=f32
+            ) * unit
+
+        last = pl.multiple_of((source // 2) * 512, 512)
+        s = scores(last)
+        row_id = source * 256 + lax.broadcasted_iota(i32, (256, 512), 0)
+        key_id = last + lax.broadcasted_iota(i32, (256, 512), 1)
+        s = jnp.where(key_id <= row_id, s, masked_score)
+        top = jnp.max(s, axis=-1, keepdims=True)
+        p = jnp.exp(s - top).astype(bf16)
+        acc = jnp.dot(p, vals[pl.ds(last, 512), :], preferred_element_type=f32)
+
+        def step(i, carry):
+            top, acc = carry
+            at = pl.multiple_of(i * 512, 512)
+            s = scores(at)
+            new = jnp.maximum(top, jnp.max(s, axis=-1, keepdims=True))
+            p = jnp.exp(s - new).astype(bf16)
+            acc = acc * jnp.exp(top - new) + jnp.dot(p, vals[pl.ds(at, 512), :], preferred_element_type=f32)
+            return new, acc
+
+        top, acc = lax.fori_loop(0, source // 2, step, (top, acc))
+        attended[k] = (acc[:, 0:128] / acc[:, 128:256]).astype(bf16)
+        mine = pl.ds(pl.multiple_of(me * 128, 128), 128)
+
+        @pl.when(k > 0)
+        def _():
+            remote(attended.at[k], heads.at[:, mine], so.at[k], ro.at[k], source).start()
+
+        @pl.when(k == 0)
+        def _():
+            heads[:, mine] = attended[0]
+
+        return 0
+
+    lax.fori_loop(0, 16, one_block, 0)
+    for d in (1, 2, 3):
+        to_x(3)[d - 1].wait_recv()
+        to_core(3, d).start()
+    backs = [None]
+    for k in range(1, 16):
+        source = along((4 - ORDER[k][0]) % 4, (4 - ORDER[k][1]) % 4)
+        mine = pl.ds(pl.multiple_of(me * 128, 128), 128)
+        backs.append(remote(attended.at[k], heads.at[:, mine], so.at[k], ro.at[k], source))
+    for k in range(1, 16):
+        backs[k].wait_recv()
+    for g in range(4):
+        for d in range(4):
+            to_core(g, d).wait_recv()
 
     @pl.loop(0, 8)
     def _(n):
         cols = pl.ds(pl.multiple_of(n * 256, 256), 256)
-        p = jnp.dot(heads[...], wo[:, cols], preferred_element_type=f32).astype(bf16)
+        p = jnp.dot(heads[...], wo[n].reshape(2048, 256), preferred_element_type=f32).astype(bf16)
         after[:, cols] = resid[:, cols].astype(f32) + p.astype(f32)
 
     @pl.loop(0, 8)
@@ -117,8 +292,6 @@
         owner = [shifted(me, *ORDER[4 * g + j]) * 64 for j in range(4)]
         base = jnp.where(r < 64, owner[0], jnp.where(r < 128, owner[1], jnp.where(r < 192, owner[2], owner[3])))
         return base + (r & 63)
-
-    pl.semaphore_wait(barrier, 15)
 
     first = [
         None if k == 0 else remote(outgoing.at[k], arrived.at[k], send1.at[k], recv1.at[k], shifted(me, *ORDER[k]))
@@ -187,16 +360,22 @@
     for k in range(1, 16):
         first[k].wait_send()
         second[k].wait_send()
-
-
-def experts(heads, wo, resid, gain, routes, weight, wg, wu, wd):
+    for c in a1 + b1 + w1 + a2 + b2 + w2 + asks[1:] + backs[1:]:
+        c.wait_send()
+    for g in range(4):
+        for c in to_x(g) + [to_core(g, d) for d in range(4)]:
+            c.wait_send()
+
+
+def layer(q_slab, lat_a, lat_b, up_kv, wo, resid, gain, routes, weight, wg, wu, wd):
     v, a = pl.BlockSpec(memory_space=pltpu.VMEM), pl.BlockSpec(memory_space=pl.ANY)
     bf16, f32 = jnp.bfloat16, jnp.float32
+    dma = pltpu.SemaphoreType.DMA
     return pl.pallas_call(
-        experts_kernel,
-        name="experts",
+        layer_kernel,
+        name="layer",
         out_shape=jax.ShapeDtypeStruct((256, 2048), bf16),
-        in_specs=[v] * 7 + [a] * 3,
+        in_specs=[a, a, a, v, a] + [v] * 5 + [a] * 3,
         out_specs=v,
         scratch_shapes=[
             pltpu.VMEM((2048, 1024), bf16),
@@ -210,13 +389,26 @@
             pltpu.VMEM((16, 64, 2048), bf16),
             pltpu.VMEM((16, 64, 2048), bf16),
             pltpu.VMEM((256, 2048), f32),
-            pltpu.SemaphoreType.DMA((3,)),
+            pltpu.VMEM((16, 384, 128), bf16),
+            pltpu.VMEM((4, 4, 256, 128), bf16),
+            pltpu.VMEM((4, 4, 384, 128), bf16),
+            pltpu.VMEM((4096, 256), bf16),
+            pltpu.VMEM((4096, 256), bf16),
+            pltpu.VMEM((256, 256), bf16),
+            pltpu.VMEM((16, 256, 128), bf16),
+            pltpu.VMEM((256, 2048), bf16),
+            pltpu.VMEM((8, 4, 4, 128, 256), bf16),
+            dma((3,)),
         ]
-        + [pltpu.SemaphoreType.DMA((16,))] * 4,
+        + [dma((16,))] * 4
+        + [dma((4,))] * 9
+        + [dma((16,))] * 4
+        + [dma((4,))] * 4
+        + [dma((4, 4))] * 4,
         compiler_params=pltpu.CompilerParams(
-            collective_id=1, has_side_effects=True, vmem_limit_bytes=60 * 1024 * 1024
+            collective_id=1, has_side_effects=True, vmem_limit_bytes=65400 * 1024
         ),
-    )(heads, wo, resid, gain, routes, routes.T, weight, wg, wu, wd)
+    )(q_slab, lat_a, lat_b, up_kv, wo, resid, gain, routes, routes.T, weight, wg, wu, wd)
 
 
 def shards(
@@ -236,68 +428,20 @@
     routes,
     route_weight,
 ):
-    tokens_here = latent.shape[1]
-    sp_count = lax.axis_size("sp")
-    length = tokens_here * sp_count
-    block = min(512, length)
-    blocks = length // block
-    local_pos = lax.axis_index("sp") * tokens_here + jnp.arange(tokens_here, dtype=jnp.int32)
+    tokens = latent.shape[1]
+    local_pos = lax.axis_index("sp") * tokens + jnp.arange(tokens, dtype=jnp.int32)
     latent_normed = rms_scaled(latent[0], latent_gain).astype(jnp.bfloat16)
     key_turned = rotate(key_rope[0], local_pos)
     query_turned = rotate(query_rope[0], local_pos)
-    all_latent, all_keyturn = sent_together((latent_normed, key_turned), "sp", 0, 1)
-    query_plain, query_turn = (
-        lax.all_to_all(query_nope[0], "sp", split_axis=1, concat_axis=0, tiled=True),
-        lax.all_to_all(query_turned, "sp", split_axis=1, concat_axis=0, tiled=True),
-    )
-    heads_here = query_plain.shape[1]
-    key_plain = (
-        jnp.dot(all_latent, key_up, preferred_element_type=jnp.float32)
-        .astype(jnp.bfloat16)
-        .reshape(length, heads_here, -1)
-    )
-    value_heads = (
-        jnp.dot(all_latent, value_up, preferred_element_type=jnp.float32)
-        .astype(jnp.bfloat16)
-        .reshape(length, heads_here, -1)
-    )
-    scale = (query_plain.shape[-1] + query_turn.shape[-1]) ** (-0.5)
-    key_ids = jnp.arange(length, dtype=jnp.int32)
-
-    def one_block(items):
-        index, plain_block, turn_block = items
-        scores = jnp.einsum(
-            "bhd,shd->hbs", plain_block, key_plain, preferred_element_type=jnp.float32
-        )
-        scores = (
-            scores
-            + jnp.einsum("bhr,sr->hbs", turn_block, all_keyturn, preferred_element_type=jnp.float32)
-        ) * scale
-        row_ids = index * block + jnp.arange(block, dtype=jnp.int32)
-        allowed = key_ids[None, :] <= row_ids[:, None]
-        scores = jnp.where(allowed[None], scores, masked_score)
-        largest = jnp.max(scores, axis=-1, keepdims=True)
-        powers = jnp.exp(scores - largest)
-        attend = (powers / jnp.sum(powers, axis=-1, keepdims=True)).astype(jnp.bfloat16)
-        return jnp.einsum(
-            "hbs,shd->bhd", attend, value_heads, preferred_element_type=jnp.float32
-        ).astype(jnp.bfloat16)
-
-    attended = lax.map(
-        one_block,
-        (
-            jnp.arange(blocks, dtype=jnp.int32),
-            query_plain.reshape(blocks, block, heads_here, -1),
-            query_turn.reshape(blocks, block, heads_here, -1),
-        ),
-    )
-    attended = attended.reshape(length, heads_here, -1)
-    token_heads = lax.all_to_all(attended, "sp", split_axis=0, concat_axis=1, tiled=True)
-    flat_heads = token_heads.reshape(tokens_here, -1)
-    head_rows = lax.all_gather(out_proj, "dp", axis=1, tiled=True)
-    wo = lax.all_gather(head_rows, "sp", axis=0, tiled=True)
-    return experts(
-        flat_heads, wo, resid[0], norm_gain[None], routes[0], route_weight[0],
+    half = tokens // 2
+    turned = query_turned.reshape(2, half, 16, 64).transpose(2, 1, 0, 3).reshape(16, half, 128)
+    q_slab = jnp.concatenate([query_nope[0].transpose(1, 0, 2), turned], axis=1)
+    key_pack = jnp.concatenate([key_turned[:half], key_turned[half:]], axis=1)
+    lat_a = latent_normed[:, :128]
+    lat_b = jnp.concatenate([latent_normed[:, 128:], key_pack], axis=0)
+    up_kv = jnp.concatenate([key_up, value_up], axis=1)
+    return layer(
+        q_slab, lat_a, lat_b, up_kv, out_proj, resid[0], norm_gain[None], routes[0], route_weight[0],
         expert_gate[0], expert_up[0], expert_down[0],
     )[None]
 

time: 323 us -> 240 us (0.74)
  the two profiles are of different devices: /device:TPU:20 before, /device:TPU:0 now
where the time goes in v2:
time: 240 us; the launch traced here: 238 us
  Pallas kernels  226 us (94%)
  local copies, waits for them, and re-layouts  6.38 us (3%)
  other arithmetic  5.55 us (2%)
    pallas_call x1, Pallas kernels, layer(): pl.pallas_call(layer_kernel, name='layer', out_shape=jax.ShapeDtypeStruct...  226 us

profile of v2, /device:TPU:0, one launch (start us, length us, event | category | flops | bytes accessed | tf_op | source)
XLA Modules:
  0.0 238.1 jit_solution(792309472813922215)
XLA Ops:
  0.0 1.1 bitcast_convert_fusion
  1.1 0.9 copy.45
  2.1 0.6 subtract_convert_fusion.1
  2.7 0.0 copy-start
  2.7 0.1 copy.42
  2.7 0.1 copy.41
  2.8 0.2 subtract_convert_fusion
  3.0 0.1 concatenate.26
  3.1 0.1 concatenate.25
  3.1 0.7 maximum_bitcast_fusion
  3.8 0.1 copy.43
  4.0 0.3 copy.44
  4.3 0.3 copy.49
  4.6 1.3 pad_maximum_fusion.q_in_hbm
  5.8 0.1 fusion
  6.0 0.1 fusion.2
  6.1 0.6 fusion.12
  6.7 0.1 fusion.11
  6.8 0.7 fusion.10.lat_b
  7.5 0.7 pad_maximum_fusion.1.up_kv
  8.2 0.8 copy.47.routes
  9.0 0.8 copy.46
  9.8 225.9 %layer.1 = bf16[256,2048]{1,0:T(8,128)(2,1)} custom-call(bf16[16,384,128]{2,1,0:T(8,128)(2,1)} %pad_maximum_fusion.q_in_hbm, bf16[256,128]{1,0:T(8,128)(2,1)} %get-tuple-element.10.lat_a, bf16[384,128]{1,0:T(8,128)(2,1)} %fusion.10.lat_b, bf16[256,256]{1,0:T(8,128)(2,1)} %pad_maximum_fusion.1.up_kv, bf16[128,256]{1,0:T(8,128)(2,1)} %wo_hbm.1, ...), custom_call_target="tpu_custom_call" | custom-call | tf_op jit(solution)/shard_map/layer/pallas_call | solution.py:374
  235.7 2.3 copy.51
  (17 shorter events, 0.1 us)
Async XLA Ops:
  2.7 1.6 copy-start
  3.9 1.9 copy-start.1
  4.0 2.0 copy-start.6
  4.3 3.3 %copy-start.2 = (bf16[256,128]{1,0:T(8,128)(2,1)S(1)}, bf16[256,128]{1,0:T(8,128)(2,1)}, u32[]{:S(2)}) copy-start(bf16[256,128]{1,0:T(8,128)(2,1)} %param.22) | copy-start | bytes 196612
  4.3 3.3 %copy-start.3 = (bf16[256,128]{1,0:T(8,128)(2,1)S(1)}, bf16[256,128]{1,0:T(8,128)(2,1)}, u32[]{:S(2)}) copy-start(bf16[256,128]{1,0:T(8,128)(2,1)} %param.21) | copy-start | bytes 196612
  4.3 3.9 %copy-start.4 = (s32[1,256,2]{1,2,0:T(2,128)S(1)}, s32[1,256,2]{1,2,0:T(2,128)}, u32[]{:S(2)}) copy-start(s32[1,256,2]{1,2,0:T(2,128)} %param.28) | copy-start | bytes 6148
  4.3 4.7 %copy-start.5 = (f32[1,256,2]{1,2,0:T(2,128)S(1)}, f32[1,256,2]{1,2,0:T(2,128)}, u32[]{:S(2)}) copy-start(f32[1,256,2]{1,2,0:T(2,128)} %param.29) | copy-start | bytes 6148

commit v3 on v2

--- a/solution.py
+++ b/solution.py
@@ -1,3 +1,5 @@
+import math
+
 import jax
 import jax.numpy as jnp
 from jax import lax
@@ -46,7 +48,8 @@
     return value - (1 << 32) if value >= 1 << 31 else value
 
 
-ZS, YS = packed([o[0] for o in ORDER]), packed([o[1] for o in ORDER])
+PAIRS = [(0, 0), (2, 1), (1, 1), (3, 1), (2, 0), (0, 1), (1, 0), (3, 0)]
+PZ, PJ = packed([o[0] for o in PAIRS]), packed([o[1] for o in PAIRS])
 
 
 def shifted(me, dz, dy):
@@ -66,9 +69,9 @@
 
 
 def layer_kernel(
-    q_in_hbm, lat_a, lat_b, up_kv, wo_hbm, resid, gain, routes, routes_t, weight, wg_hbm, wu_hbm, wd_hbm, out,
+    q_in_hbm, lat_a, lat_b, up_k, up_vt, wo_hbm, resid, gain, routes, routes_t, weight, wg_hbm, wu_hbm, wd_hbm, out,
     wg, wu, wd, after, normed, outgoing, arrived, hidden, result, returned, total,
-    q_in, la, lb, keys, vals, q_cat, attended, heads, wo,
+    q_in, la, lb, keys, vals, attended, heads, wo,
     wsem, send1, recv1, send2, recv2,
     lsem, sa1, ra1, sb1, rb1, sa2, ra2, sb2, rb2, sq, rq, so, ro, swz, rwz, swy, rwy, swx, rwx, swc, rwc,
 ):
@@ -86,7 +89,7 @@
         pl.semaphore_signal(barrier, inc=1, device_id={"dp": t}, device_id_type=MESH)
     fill_wo = pltpu.make_async_copy(wo_hbm, wo.at[dp, z, y], lsem.at[0])
     fill_wo.start()
-    fill_q = pltpu.make_async_copy(q_in_hbm.at[me], q_in.at[0], lsem.at[1])
+    fill_q = pltpu.make_async_copy(q_in_hbm.at[me], q_in.at[me], lsem.at[1])
     fill_q.start()
     fill_a = pltpu.make_async_copy(lat_a, la.at[z, y], lsem.at[2])
     fill_a.start()
@@ -112,10 +115,16 @@
     a2 = [remote(la.at[:, y], la.at[:, y], sa2.at[d], ra2.at[d], along(0, d)) for d in (1, 2, 3)]
     b2 = [remote(lb.at[z], lb.at[z], sb2.at[d], rb2.at[d], along(d, 0)) for d in (1, 2, 3)]
     w2 = [remote(wo.at[dp, :, y], wo.at[dp, :, y], swy.at[d], rwy.at[d], along(0, d)) for d in (1, 2, 3)]
-    asks = [
-        None if k == 0 else remote(q_in_hbm.at[along(*ORDER[k])], q_in.at[k], sq.at[k], rq.at[k], along(*ORDER[k]))
-        for k in range(16)
-    ]
+    asks = []
+    for r, (dz, dj) in enumerate(PAIRS):
+        for e in range(2):
+            if r == 0:
+                target = me + 1 - 2 * lax.rem(y, 2)
+                if e == 1:
+                    continue
+            else:
+                target = lax.rem(z + 4 - dz, 4) * 4 + lax.rem(y // 2 + dj, 2) * 2 + e
+            asks.append(remote(q_in_hbm.at[target], q_in.at[me], sq.at[2 * r + e], rq.at[me], target))
 
     def to_x(g):
         part = wo.at[dp, :, lax.rem(y + 4 - g, 4)]
@@ -135,7 +144,11 @@
             device_id={"dp": other}, device_id_type=MESH,
         )
 
-    for c in a1 + b1 + w1:
+    for c in w1 + a1 + b1:
+        c.start()
+    for c in w1:
+        c.wait_recv()
+    for c in w2 + to_x(0) + [to_core(0, 0)]:
         c.start()
     for c in a1:
         c.wait_recv()
@@ -143,16 +156,14 @@
         c.start()
     for c in b1:
         c.wait_recv()
-    for c in b2:
+    for c in b2 + asks:
         c.start()
-    for c in w1:
-        c.wait_recv()
-    for c in w2 + to_x(0) + [to_core(0, 0)]:
-        c.start()
-    for c in asks[1:]:
-        c.start()
-
-    vals[:, 128:256] = jnp.ones((4096, 128), bf16)
+    for g in (1, 2, 3):
+        w2[g - 1].wait_recv()
+        for c in to_x(g) + [to_core(g, 0)]:
+            c.start()
+
+    vals[128:144, :] = jnp.ones((16, 4096), bf16)
     for c in a2 + b2:
         c.wait_recv()
 
@@ -161,9 +172,10 @@
         bz, by = b // 4, lax.rem(b, 4)
         rows = pl.ds(pl.multiple_of(b * 256, 256), 256)
         lat = jnp.concatenate([la[bz, by], lb[bz, by, 0:256, :]], axis=1)
-        kv = jnp.dot(lat, up_kv[...], preferred_element_type=f32).astype(bf16)
-        keys[rows, 0:128] = kv[:, 0:128]
-        vals[rows, 0:128] = kv[:, 128:256]
+        keys[rows, 0:128] = jnp.dot(lat, up_k[...], preferred_element_type=f32).astype(bf16)
+        vals[0:128, rows] = lax.dot_general(
+            up_vt[...], lat, (((1,), (1,)), ((), ())), preferred_element_type=f32
+        ).astype(bf16)
         turn = lb[bz, by, 256:384, :].astype(f32)
         swap = pltpu.roll(turn, 64, 1)
         low = lax.broadcasted_iota(i32, (128, 128), 1) < 64
@@ -172,88 +184,83 @@
         keys[pl.ds(pl.multiple_of(start + 128, 128), 128), 128:256] = jnp.where(low, swap, turn).astype(bf16)
 
     fill_q.wait()
-    unit = 192.0 ** -0.5
-
-    def one_block(k, _):
-        dz, dy = (ZS >> (2 * k)) & 3, (YS >> (2 * k)) & 3
-        source = shifted(me, 4 - dz, 4 - dy)
-
-        @pl.when(k > 0)
-        def _():
-            remote(q_in.at[k], q_in.at[k], sq.at[k], rq.at[k], source).wait_recv()
-
-        for g in (1, 2, 3):
-
-            @pl.when(k == 4 * g - 2)
-            def _(g=g):
-                w2[g - 1].wait_recv()
-                for c in to_x(g) + [to_core(g, 0)]:
-                    c.start()
+    unit = 192.0 ** -0.5 * math.log2(math.e)
+    mine = pl.ds(pl.multiple_of(me * 128, 128), 128)
+
+    def one_pair(r, _):
+        dz, dj = (PZ >> (2 * r)) & 3, (PJ >> (2 * r)) & 3
+        pair = lax.rem(z + dz, 4) * 2 + lax.rem(y // 2 + dj, 2)
+        for e in range(2):
+            source = 2 * pair + e
+
+            @pl.when(source != me)
+            def _(source=source):
+                remote(q_in.at[source], q_in.at[source], sq.at[0], rq.at[source], source).wait_recv()
 
         for g in (0, 1, 2):
 
-            @pl.when(k == 5 * g + 5)
+            @pl.when(r == 2 * g + 2)
             def _(g=g):
                 for d in (1, 2, 3):
                     to_x(g)[d - 1].wait_recv()
                     to_core(g, d).start()
 
-        q_cat[:, 0:128] = q_in[k, 0:256, :]
-        turn = q_in[k, 256:384, :]
-        low = lax.broadcasted_iota(i32, (128, 128), 1) < 64
-        zero = jnp.zeros((128, 128), bf16)
-        q_cat[0:128, 128:256] = jnp.where(low, turn, zero)
-        q_cat[128:256, 128:256] = jnp.where(low, zero, turn)
-        q = q_cat[...]
+        q = jnp.concatenate([q_in[2 * pair], q_in[2 * pair + 1]], axis=1)
 
         def scores(at):
-            return lax.dot_general(
-                q, keys[pl.ds(at, 512), :], (((1,), (1,)), ((), ())), preferred_element_type=f32
-            ) * unit
-
-        last = pl.multiple_of((source // 2) * 512, 512)
-        s = scores(last)
-        row_id = source * 256 + lax.broadcasted_iota(i32, (256, 512), 0)
-        key_id = last + lax.broadcasted_iota(i32, (256, 512), 1)
-        s = jnp.where(key_id <= row_id, s, masked_score)
-        top = jnp.max(s, axis=-1, keepdims=True)
-        p = jnp.exp(s - top).astype(bf16)
-        acc = jnp.dot(p, vals[pl.ds(last, 512), :], preferred_element_type=f32)
-
-        def step(i, carry):
-            top, acc = carry
-            at = pl.multiple_of(i * 512, 512)
-            s = scores(at)
-            new = jnp.maximum(top, jnp.max(s, axis=-1, keepdims=True))
-            p = jnp.exp(s - new).astype(bf16)
-            acc = acc * jnp.exp(top - new) + jnp.dot(p, vals[pl.ds(at, 512), :], preferred_element_type=f32)
-            return new, acc
-
-        top, acc = lax.fori_loop(0, source // 2, step, (top, acc))
-        attended[k] = (acc[:, 0:128] / acc[:, 128:256]).astype(bf16)
-        mine = pl.ds(pl.multiple_of(me * 128, 128), 128)
-
-        @pl.when(k > 0)
-        def _():
-            remote(attended.at[k], heads.at[:, mine], so.at[k], ro.at[k], source).start()
-
-        @pl.when(k == 0)
-        def _():
-            heads[:, mine] = attended[0]
+            return jnp.dot(keys[pl.ds(at, 512), 0:192], q, preferred_element_type=f32)
+
+        def weigh(s, at, top, acc):
+            new = jnp.maximum(top, jnp.max(s, axis=0, keepdims=True) * unit)
+            p = jnp.exp2(s * unit - new).astype(bf16)
+            return new, acc * jnp.exp2(top - new) + jnp.dot(
+                vals[:, pl.ds(at, 512)], p, preferred_element_type=f32
+            )
+
+        last = pl.multiple_of(pair * 512, 512)
+        key_id = lax.broadcasted_iota(i32, (512, 512), 0)
+        row_id = lax.broadcasted_iota(i32, (512, 512), 1)
+        s = jnp.where(key_id <= row_id, scores(last), masked_score)
+        top = jnp.max(s, axis=0, keepdims=True) * unit
+        p = jnp.exp2(s * unit - top).astype(bf16)
+        acc = jnp.dot(vals[:, pl.ds(last, 512)], p, preferred_element_type=f32)
+
+        def single(i, carry):
+            at = pl.multiple_of((pair - 1) * 512, 512)
+            return weigh(scores(at), at, *carry)
+
+        def double(i, carry):
+            at = pl.multiple_of(i * 1024, 1024)
+            then = pl.multiple_of(at + 512, 512)
+            s, t = scores(at), scores(then)
+            return weigh(t, then, *weigh(s, at, *carry))
+
+        carry = lax.fori_loop(0, lax.rem(pair, 2), single, (top, acc))
+        top, acc = lax.fori_loop(0, pair // 2, double, carry)
+        rows = acc[0:128] / acc[128:129]
+        for e in range(2):
+            attended[2 * r + e] = rows[:, 256 * e : 256 * e + 256].T.astype(bf16)
+        for e in range(2):
+            source = 2 * pair + e
+
+            @pl.when(source != me)
+            def _(e=e, source=source):
+                remote(attended.at[2 * r + e], heads.at[:, mine], so.at[2 * r + e], ro.at[me], source).start()
+
+            @pl.when(source == me)
+            def _(e=e):
+                heads[:, mine] = attended[2 * r + e]
 
         return 0
 
-    lax.fori_loop(0, 16, one_block, 0)
+    lax.fori_loop(0, 8, one_pair, 0)
     for d in (1, 2, 3):
         to_x(3)[d - 1].wait_recv()
         to_core(3, d).start()
-    backs = [None]
     for k in range(1, 16):
-        source = along((4 - ORDER[k][0]) % 4, (4 - ORDER[k][1]) % 4)
-        mine = pl.ds(pl.multiple_of(me * 128, 128), 128)
-        backs.append(remote(attended.at[k], heads.at[:, mine], so.at[k], ro.at[k], source))
-    for k in range(1, 16):
-        backs[k].wait_recv()
+        head = along(*ORDER[k])
+        there = pl.ds(pl.multiple_of(head * 128, 128), 128)
+        remote(attended.at[0], heads.at[:, there], so.at[0], ro.at[head], head).wait_recv()
     for g in range(4):
         for d in range(4):
             to_core(g, d).wait_recv()
@@ -360,14 +367,20 @@
     for k in range(1, 16):
         first[k].wait_send()
         second[k].wait_send()
-    for c in a1 + b1 + w1 + a2 + b2 + w2 + asks[1:] + backs[1:]:
+    for c in a1 + b1 + w1 + a2 + b2 + w2 + asks:
         c.wait_send()
+    for n in range(16):
+
+        @pl.when(lax.rem(y, 2) != n)
+        def _(n=n):
+            remote(attended.at[n], heads.at[:, mine], so.at[n], ro.at[me], me).wait_send()
+
     for g in range(4):
         for c in to_x(g) + [to_core(g, d) for d in range(4)]:
             c.wait_send()
 
 
-def layer(q_slab, lat_a, lat_b, up_kv, wo, resid, gain, routes, weight, wg, wu, wd):
+def layer(q_slab, lat_a, lat_b, up_k, up_vt, wo, resid, gain, routes, weight, wg, wu, wd):
     v, a = pl.BlockSpec(memory_space=pltpu.VMEM), pl.BlockSpec(memory_space=pl.ANY)
     bf16, f32 = jnp.bfloat16, jnp.float32
     dma = pltpu.SemaphoreType.DMA
@@ -375,7 +388,7 @@
         layer_kernel,
         name="layer",
         out_shape=jax.ShapeDtypeStruct((256, 2048), bf16),
-        in_specs=[a, a, a, v, a] + [v] * 5 + [a] * 3,
+        in_specs=[a, a, a, v, v, a] + [v] * 5 + [a] * 3,
         out_specs=v,
         scratch_shapes=[
             pltpu.VMEM((2048, 1024), bf16),
@@ -389,12 +402,11 @@
             pltpu.VMEM((16, 64, 2048), bf16),
             pltpu.VMEM((16, 64, 2048), bf16),
             pltpu.VMEM((256, 2048), f32),
-            pltpu.VMEM((16, 384, 128), bf16),
+            pltpu.VMEM((16, 192, 256), bf16),
             pltpu.VMEM((4, 4, 256, 128), bf16),
             pltpu.VMEM((4, 4, 384, 128), bf16),
             pltpu.VMEM((4096, 256), bf16),
-            pltpu.VMEM((4096, 256), bf16),
-            pltpu.VMEM((256, 256), bf16),
+            pltpu.VMEM((144, 4096), bf16),
             pltpu.VMEM((16, 256, 128), bf16),
             pltpu.VMEM((256, 2048), bf16),
             pltpu.VMEM((8, 4, 4, 128, 256), bf16),
@@ -408,7 +420,7 @@
         compiler_params=pltpu.CompilerParams(
             collective_id=1, has_side_effects=True, vmem_limit_bytes=65400 * 1024
         ),
-    )(q_slab, lat_a, lat_b, up_kv, wo, resid, gain, routes, routes.T, weight, wg, wu, wd)
+    )(q_slab, lat_a, lat_b, up_k, up_vt, wo, resid, gain, routes, routes.T, weight, wg, wu, wd)
 
 
 def shards(
@@ -434,14 +446,14 @@
     key_turned = rotate(key_rope[0], local_pos)
     query_turned = rotate(query_rope[0], local_pos)
     half = tokens // 2
-    turned = query_turned.reshape(2, half, 16, 64).transpose(2, 1, 0, 3).reshape(16, half, 128)
-    q_slab = jnp.concatenate([query_nope[0].transpose(1, 0, 2), turned], axis=1)
+    q_slab = jnp.concatenate(
+        [query_nope[0].transpose(1, 2, 0), query_turned.transpose(1, 2, 0)], axis=1
+    )
     key_pack = jnp.concatenate([key_turned[:half], key_turned[half:]], axis=1)
     lat_a = latent_normed[:, :128]
     lat_b = jnp.concatenate([latent_normed[:, 128:], key_pack], axis=0)
-    up_kv = jnp.concatenate([key_up, value_up], axis=1)
     return layer(
-        q_slab, lat_a, lat_b, up_kv, out_proj, resid[0], norm_gain[None], routes[0], route_weight[0],
+        q_slab, lat_a, lat_b, key_up, value_up.T, out_proj, resid[0], norm_gain[None], routes[0], route_weight[0],
         expert_gate[0], expert_up[0], expert_down[0],
     )[None]
 

time: 240 us -> 215 us (0.90)
  Pallas kernels: 226 us -> 200 us
    pallas_call x1, Pallas kernels: 226 us -> 200 us  [layer(): pl.pallas_call(layer_kernel, name='layer', out_shape=jax.ShapeDtypeStruct...]
    unnamed x18 -> x17, local copies, waits for them, and re-layouts: 4.28 us -> 5.56 us
where the time goes in v3:
time: 215 us; the launch traced here: 212 us
  Pallas kernels  200 us (93%)
  local copies, waits for them, and re-layouts  7.12 us (3%)
  other arithmetic  4.33 us (2%)
    pallas_call x1, Pallas kernels, layer(): pl.pallas_call(layer_kernel, name='layer', out_shape=jax.ShapeDtypeStruct...  200 us
    unnamed x17, local copies, waits for them, and re-layouts  5.56 us

profile of v3, /device:TPU:0, one launch (start us, length us, event | category | flops | bytes accessed | tf_op | source)
XLA Modules:
  0.0 211.7 jit_solution(10233095581380670340)
XLA Ops:
  0.0 1.2 bitcast_convert_fusion
  1.2 0.9 copy.27
  2.2 0.6 subtract_convert_fusion.1
  2.8 0.1 copy.26
  2.8 0.1 copy.25
  2.9 0.2 subtract_convert_fusion
  3.1 0.0 copy-start.1
  3.1 0.0 copy-start.5
  3.1 0.0 copy-done
  3.1 0.0 copy-start.2
  3.2 0.0 copy-start.3
  3.2 0.0 copy-start.4
  3.2 0.8 copy.23
  4.0 1.3 pad_maximum_fusion.q_in_hbm
  5.2 0.1 fusion
  5.4 0.1 fusion.2
  5.5 0.6 fusion.12
  6.1 0.1 fusion.11
  6.2 0.7 fusion.10.lat_b
  6.9 0.7 copy.28
  7.7 0.8 copy.30.routes
  8.5 0.8 copy.29
  9.3 200.1 %layer.1 = bf16[256,2048]{1,0:T(8,128)(2,1)} custom-call(bf16[16,192,256]{2,1,0:T(8,128)(2,1)} %pad_maximum_fusion.q_in_hbm, bf16[256,128]{1,0:T(8,128)(2,1)} %get-tuple-element.10.lat_a, bf16[384,128]{1,0:T(8,128)(2,1)} %fusion.10.lat_b, bf16[256,128]{1,0:T(8,128)(2,1)} %up_k.1, bf16[128,256]{1,0:T(8,128)(2,1)} %bitcast.33, bf16[128,256]{1,0:T(8,128)(2,1)} %wo_hbm.1, ...), custom_call_target="tpu_custom_call" | custom-call | tf_op jit(solution)/shard_map/layer/pallas_call | solution.py:387
  209.4 2.3 %copy.32 = bf16[1,256,2048]{2,1,0:T(8,128)(2,1)} copy(bf16[1,256,2048]{2,1,0:T(8,128)(2,1)} %bitcast.26) | data formatting | bytes 2097152
  (11 shorter events, 0.1 us)
Async XLA Ops:
  0.0 3.1 %copy-start = (bf16[1,256,16,128]{3,2,1,0:T(8,128)(2,1)S(1)}, bf16[1,256,16,128]{3,2,1,0:T(8,128)(2,1)}, u32[]{:S(2)}) copy-start(bf16[1,256,16,128]{3,2,1,0:T(8,128)(2,1)} %param.15) | copy-start | bytes 3145732
  3.1 2.2 %copy-start.1 = (bf16[1,256,256]{2,1,0:T(8,128)(2,1)S(1)}, bf16[1,256,256]{2,1,0:T(8,128)(2,1)}, u32[]{:S(2)}) copy-start(bf16[1,256,256]{2,1,0:T(8,128)(2,1)} %param.17) | copy-start | bytes 393220
  3.1 2.3 %copy-start.5 = (f32[256]{0:T(256)S(1)}, f32[256]{0:T(256)}, u32[]{:S(2)}) copy-start(f32[256]{0:T(256)} %param.20) | copy-start | bytes 3076
  3.1 3.8 %copy-start.2 = (bf16[256,128]{1,0:T(8,128)(2,1)S(1)}, bf16[256,128]{1,0:T(8,128)(2,1)}, u32[]{:S(2)}) copy-start(bf16[256,128]{1,0:T(8,128)(2,1)} %param.22) | copy-start | bytes 196612
  3.2 4.5 %copy-start.3 = (s32[1,256,2]{1,2,0:T(2,128)S(1)}, s32[1,256,2]{1,2,0:T(2,128)}, u32[]{:S(2)}) copy-start(s32[1,256,2]{1,2,0:T(2,128)} %param.28) | copy-start | bytes 6148
  3.2 5.3 %copy-start.4 = (f32[1,256,2]{1,2,0:T(2,128)S(1)}, f32[1,256,2]{1,2,0:T(2,128)}, u32[]{:S(2)}) copy-start(f32[1,256,2]{1,2,0:T(2,128)} %param.29) | copy-start | bytes 6148

commit v4 on v3

--- a/solution.py
+++ b/solution.py
@@ -48,6 +48,8 @@
     return value - (1 << 32) if value >= 1 << 31 else value
 
 
+PLACE = {0: 0, 1: 1, 3: 2, 2: 3}
+SHIFT = [0, 1, 3, 2]
 PAIRS = [(0, 0), (2, 1), (1, 1), (3, 1), (2, 0), (0, 1), (1, 0), (3, 0)]
 PZ, PJ = packed([o[0] for o in PAIRS]), packed([o[1] for o in PAIRS])
 
@@ -69,10 +71,10 @@
 
 
 def layer_kernel(
-    q_in_hbm, lat_a, lat_b, up_k, up_vt, wo_hbm, resid, gain, routes, routes_t, weight, wg_hbm, wu_hbm, wd_hbm, out,
-    wg, wu, wd, after, normed, outgoing, arrived, hidden, result, returned, total,
+    q_in_hbm, lat_a, lat_b, up_k, up_vt, wo_hbm, resid, gain, told_in, wg_hbm, wu_hbm, wd_hbm, out,
+    wg, wu, wd, after, told_all, shared, outgoing, arrived, hidden, result, returned, final,
     q_in, la, lb, keys, vals, attended, heads, wo,
-    wsem, send1, recv1, send2, recv2,
+    wsem, st, rt, ssh, rsh, sd, rd, sg, rg, sf, rf,
     lsem, sa1, ra1, sb1, rb1, sa2, ra2, sb2, rb2, sq, rq, so, ro, swz, rwz, swy, rwy, swx, rwx, swc, rwc,
 ):
     me, dp = lax.axis_index("sp"), lax.axis_index("dp")
@@ -101,6 +103,16 @@
     ]
     for load in loads:
         load.start()
+    tok = lax.broadcasted_iota(i32, (256, 256), 0)
+    tok_l = lax.broadcasted_iota(i32, (256, 256), 1)
+    upper = jnp.where(tok < tok_l, 1.0, 0.0).astype(bf16)
+    expert = lax.broadcasted_iota(i32, (16, 256), 0).astype(f32)
+    hot = [jnp.where(expert == told_in[k : k + 1, :], 1.0, 0.0) for k in range(2)]
+    before = jnp.dot((hot[0] + hot[1]).astype(bf16), upper, preferred_element_type=f32) + expert * 64.0
+    for h in range(2):
+        for k in range(2):
+            told_all[h, 0, k : k + 1, :] = jnp.sum(hot[k] * before, axis=0, keepdims=True)
+        told_all[h, 0, 2:8, :] = told_in[2:8, :]
     fill_a.wait()
     fill_b.wait()
     fill_wo.wait()
@@ -109,6 +121,11 @@
     def along(dz, dy):
         return shifted(me, dz, dy)
 
+    told = []
+    for h in range(2):
+        for d in (1, 2, 3):
+            target = along(0, d) if h == 0 else along(d, 0)
+            told.append(remote(told_all.at[h, 0], told_all.at[h, PLACE[d]], st.at[4 * h + d], rt.at[4 * h + d], target))
     a1 = [remote(la.at[z, y], la.at[z, y], sa1.at[d], ra1.at[d], along(d, 0)) for d in (1, 2, 3)]
     b1 = [remote(lb.at[z, y], lb.at[z, y], sb1.at[d], rb1.at[d], along(0, d)) for d in (1, 2, 3)]
     w1 = [remote(wo.at[dp, z, y], wo.at[dp, z, y], swz.at[d], rwz.at[d], along(d, 0)) for d in (1, 2, 3)]
@@ -156,7 +173,7 @@
         c.start()
     for c in b1:
         c.wait_recv()
-    for c in b2 + asks:
+    for c in b2 + told + asks:
         c.start()
     for g in (1, 2, 3):
         w2[g - 1].wait_recv()
@@ -276,98 +293,170 @@
         rows = pl.ds(pl.multiple_of(r * 32, 32), 32)
         a = after[rows, :]
         scale = lax.rsqrt(jnp.mean(a * a, axis=-1, keepdims=True) + epsilon)
-        normed[rows, :] = (a * scale * gain[...]).astype(bf16)
-
-    tok = lax.broadcasted_iota(i32, (256, 256), 0)
-    tok_l = lax.broadcasted_iota(i32, (256, 256), 1)
-    upper = jnp.where(tok < tok_l, 1.0, 0.0).astype(bf16)
-    lower = jnp.where(tok_l < tok, 1.0, 0.0).astype(bf16)
-    ex_t = lax.broadcasted_iota(i32, (16, 256), 0)
-    hot_t = [jnp.where(ex_t == routes_t[k : k + 1, :], 1.0, 0.0) for k in range(2)]
-    before_t = jnp.dot((hot_t[0] + hot_t[1]).astype(bf16), upper, preferred_element_type=f32)
-    base_t = before_t + (ex_t * 64).astype(f32)
-    slot_t = [jnp.sum(h * base_t, axis=0, keepdims=True).astype(i32) for h in hot_t]
-    ex_c = lax.broadcasted_iota(i32, (256, 128), 1)
-    hot_c = [jnp.where(ex_c == routes[:, k : k + 1], 1.0, 0.0) for k in range(2)]
-    before_c = jnp.dot(lower, (hot_c[0] + hot_c[1]).astype(bf16), preferred_element_type=f32)
-    base_c = before_c + (ex_c * 64).astype(f32)
-    slot_c = [jnp.sum(h * base_c, axis=1, keepdims=True).astype(i32) for h in hot_c]
-
-    def places(g, axis):
-        shape = (256, 1) if axis == 0 else (1, 256)
-        r = lax.broadcasted_iota(i32, shape, axis)
-        owner = [shifted(me, *ORDER[4 * g + j]) * 64 for j in range(4)]
+        full = (a * scale * gain[...]).astype(bf16)
+        shared[0, 0, rows, :] = full[:, 0:1024]
+        shared[1, 0, rows, :] = full[:, 1024:2048]
+
+    def line(h, d):
+        return along(0, d) if h == 0 else along(d, 0)
+
+    def cross(h, d):
+        return along(d, 0) if h == 0 else along(0, d)
+
+    def slots_of(h):
+        r = lax.broadcasted_iota(i32, (256, 1), 0)
+        owner = [cross(h, d) * 64 for d in range(4)]
         base = jnp.where(r < 64, owner[0], jnp.where(r < 128, owner[1], jnp.where(r < 192, owner[2], owner[3])))
-        return base + (r & 63)
-
-    first = [
-        None if k == 0 else remote(outgoing.at[k], arrived.at[k], send1.at[k], recv1.at[k], shifted(me, *ORDER[k]))
-        for k in range(16)
-    ]
-    for g in range(4):
-        place = places(g, 0)
-        pick = jnp.where((slot_t[0] == place) | (slot_t[1] == place), 1.0, 0.0).astype(bf16)
-        for n in range(4):
-            cols = slice(n * 512, n * 512 + 512)
-            rows = jnp.dot(pick, normed[:, cols], preferred_element_type=f32).astype(bf16)
-            for j in range(4):
-                k = 4 * g + j
-                (arrived if k == 0 else outgoing)[k, :, cols] = rows[j * 64 : j * 64 + 64]
-        if g > 0:
-            for k in range(max(1, 4 * g - 4), 4 * g):
-                first[k].start()
+        return (base + (r & 63)).astype(f32)
+
+    share = []
+    for h in range(2):
+        at = lambda n, h=h: (ssh.at[4 * h + n], rsh.at[4 * h + n])
+        share.append(
+            [
+                remote(shared.at[h, 0], shared.at[h, 1], *at(0), line(h, 1)),
+                remote(shared.at[h, 0], shared.at[h, 2], *at(1), line(h, 3)),
+                remote(shared.at[h, 1, 0:128], shared.at[h, 3, 0:128], *at(2), line(h, 1)),
+                remote(shared.at[h, 2, 128:256], shared.at[h, 3, 128:256], *at(3), line(h, 3)),
+            ]
+        )
+    for n in range(2):
+        for h in range(2):
+            share[h][n].start()
+    for c in told:
+        c.wait_recv()
     for load in loads:
         load.wait()
-    for k in range(12, 16):
-        first[k].start()
-
-    second = [
-        None if k == 0 else remote(result.at[k], returned.at[k], send2.at[k], recv2.at[k], shifted(me, (4 - ORDER[k][0]) % 4, (4 - ORDER[k][1]) % 4))
-        for k in range(16)
-    ]
-    for g in range(4):
-        for k in range(max(1, 4 * g), 4 * g + 4):
-            first[k].wait_recv()
+
+    def dealt(h, d, a):
+        there = arrived.at[0, PLACE[d], a] if h == 0 else arrived.at[1, a, PLACE[d]]
+        n = 16 * h + 4 * d + a
+        return remote(outgoing.at[h, d, a], there, sd.at[n], rd.at[n], cross(h, d))
+
+    def deal(a):
+        for h in range(2):
+            place = slots_of(h)
+            pick = (place == told_all[h, a, 0:1, :]) | (place == told_all[h, a, 1:2, :])
+            pick = jnp.where(pick, 1.0, 0.0).astype(bf16)
+            for n in range(2):
+                cols = slice(n * 512, n * 512 + 512)
+                rows = jnp.dot(pick, shared[h, a, :, cols], preferred_element_type=f32).astype(bf16)
+                if h == 0:
+                    arrived[0, 0, a, :, cols] = rows[0:64]
+                else:
+                    arrived[1, a, 0, :, cols] = rows[0:64]
+                for d in (1, 2, 3):
+                    outgoing[h, d, a, :, cols] = rows[64 * d : 64 * d + 64]
+        for d in (2, 1, 3):
+            for h in range(2):
+                dealt(h, d, a).start()
+
+    deal(0)
+    for n in range(2):
+        for h in range(2):
+            share[h][n].wait_recv()
+            share[h][n + 2].start()
+    deal(1)
+    deal(2)
+    for n in (2, 3):
+        for h in range(2):
+            share[h][n].wait_recv()
+    deal(3)
+
+    def given(h, d, a):
+        zp, yp = (PLACE[d], a) if h == 0 else (a, PLACE[d])
+        n = 16 * h + 4 * d + a
+        return remote(result.at[h, zp, yp], returned.at[h, d, a], sg.at[n], rg.at[n], cross(h, 4 - d))
+
+    for i, j in ((0, 0), (0, 1), (1, 0), (1, 1)):
+        zs, ys = (2 * i, 2 * i + 1), (2 * j, 2 * j + 1)
+        for zp in zs:
+            for yp in ys:
+                if zp > 0:
+                    dealt(0, SHIFT[zp], yp).wait_recv()
+                if yp > 0:
+                    dealt(1, SHIFT[yp], zp).wait_recv()
 
         @pl.loop(0, 4)
         def _(n):
             cols = pl.ds(pl.multiple_of(n * 256, 256), 256)
-            rows = arrived[4 * g : 4 * g + 4].reshape(256, 2048)
-            gate = jnp.dot(rows, wg[:, cols], preferred_element_type=f32)
-            up = jnp.dot(rows, wu[:, cols], preferred_element_type=f32)
+            r0 = arrived[0, 2 * i : 2 * i + 2, 2 * j : 2 * j + 2].reshape(256, 1024)
+            r1 = arrived[1, 2 * i : 2 * i + 2, 2 * j : 2 * j + 2].reshape(256, 1024)
+            gate = jnp.dot(r0, wg[0:1024, cols], preferred_element_type=f32)
+            gate = gate + jnp.dot(r1, wg[1024:2048, cols], preferred_element_type=f32)
+            up = jnp.dot(r0, wu[0:1024, cols], preferred_element_type=f32)
+            up = up + jnp.dot(r1, wu[1024:2048, cols], preferred_element_type=f32)
             hidden[:, cols] = (gate / (1.0 + jnp.exp(-gate)) * up).astype(bf16)
 
-        @pl.loop(0, 4)
-        def _(n):
-            cols = pl.ds(pl.multiple_of(n * 512, 512), 512)
-            rows = jnp.dot(hidden[...], wd[:, cols], preferred_element_type=f32).astype(bf16)
-            for j in range(4):
-                k = 4 * g + j
-                (returned if k == 0 else result)[k, :, cols] = rows[j * 64 : j * 64 + 64]
-
-        for k in range(max(1, 4 * g), 4 * g + 4):
-            second[k].start()
-
-    for g in range(4):
-        place = places(g, 1)
-        picks = [jnp.where(s == place, 1.0, 0.0).astype(bf16) for s in slot_c]
-        for k in range(max(1, 4 * g), 4 * g + 4):
-            second[k].wait_recv()
-        for n in range(4):
-            cols = slice(n * 512, n * 512 + 512)
-            rows = returned[4 * g : 4 * g + 4, :, cols].reshape(256, 512)
-            t = weight[:, 0:1] * jnp.dot(picks[0], rows, preferred_element_type=f32)
-            t = t + weight[:, 1:2] * jnp.dot(picks[1], rows, preferred_element_type=f32)
-            if g > 0:
-                t = t + total[:, cols]
-            if g < 3:
-                total[:, cols] = t
-            else:
-                out[:, cols] = (after[:, cols] + t).astype(bf16)
-    for k in range(1, 16):
-        first[k].wait_send()
-        second[k].wait_send()
-    for c in a1 + b1 + w1 + a2 + b2 + w2 + asks:
+        for h in range(2):
+
+            @pl.loop(0, 2)
+            def _(n, h=h):
+                cols = pl.ds(pl.multiple_of(n * 512, 512), 512)
+                wide = pl.ds(pl.multiple_of(n * 512 + h * 1024, 512), 512)
+                rows = jnp.dot(hidden[...], wd[:, wide], preferred_element_type=f32).astype(bf16)
+                for p, zp in enumerate(zs):
+                    for q, yp in enumerate(ys):
+                        part = rows[128 * p + 64 * q : 128 * p + 64 * q + 64]
+                        if h == 0 and zp == 0:
+                            returned[0, 0, yp, :, cols] = part
+                        elif h == 1 and yp == 0:
+                            returned[1, 0, zp, :, cols] = part
+                        else:
+                            result[h, zp, yp, :, cols] = part
+
+            for zp in zs:
+                for yp in ys:
+                    if h == 0 and zp > 0:
+                        given(0, SHIFT[zp], yp).start()
+                    if h == 1 and yp > 0:
+                        given(1, SHIFT[yp], zp).start()
+
+    for h in range(2):
+        for c in share[h]:
+            c.wait_send()
+
+    def summed(h, a):
+        n = 3 * h + a - 1
+        return remote(shared.at[h, a], final.at[h, a - 1], sf.at[n], rf.at[n], line(h, 4 - SHIFT[a]))
+
+    for a in (1, 2, 3, 0):
+        for h in range(2):
+            for d in (1, 2, 3):
+                given(h, d, a).wait_recv()
+            place = slots_of(h)
+            share_of = jnp.where(place == told_all[h, a, 0:1, :], told_all[h, a, 2:3, :], 0.0)
+            share_of = share_of + jnp.where(place == told_all[h, a, 1:2, :], told_all[h, a, 3:4, :], 0.0)
+            share_of = share_of.T
+            high = share_of.astype(bf16)
+            low = (share_of - high.astype(f32)).astype(bf16)
+            for n in range(2):
+                cols = slice(n * 512, n * 512 + 512)
+                rows = returned[h, :, a, :, cols].reshape(256, 512)
+                t = jnp.dot(high, rows, preferred_element_type=f32) + jnp.dot(low, rows, preferred_element_type=f32)
+                if a == 0:
+                    wide = slice(h * 1024 + n * 512, h * 1024 + n * 512 + 512)
+                    after[:, wide] = after[:, wide] + t
+                else:
+                    shared[h, a, :, cols] = t.astype(bf16)
+            if a > 0:
+                summed(h, a).start()
+    for h in range(2):
+        for a in (1, 2, 3):
+            summed(h, a).wait_recv()
+        wide = slice(h * 1024, h * 1024 + 1024)
+        t = after[:, wide]
+        for n in range(3):
+            t = t + final[h, n].astype(f32)
+        out[:, wide] = t.astype(bf16)
+    for h in range(2):
+        for a in range(4):
+            for d in (1, 2, 3):
+                dealt(h, d, a).wait_send()
+                given(h, d, a).wait_send()
+        for a in (1, 2, 3):
+            summed(h, a).wait_send()
+    for c in told + a1 + b1 + w1 + a2 + b2 + w2 + asks:
         c.wait_send()
     for n in range(16):
 
@@ -380,7 +469,7 @@
             c.wait_send()
 
 
-def layer(q_slab, lat_a, lat_b, up_k, up_vt, wo, resid, gain, routes, weight, wg, wu, wd):
+def layer(q_slab, lat_a, lat_b, up_k, up_vt, wo, resid, gain, told, wg, wu, wd):
     v, a = pl.BlockSpec(memory_space=pltpu.VMEM), pl.BlockSpec(memory_space=pl.ANY)
     bf16, f32 = jnp.bfloat16, jnp.float32
     dma = pltpu.SemaphoreType.DMA
@@ -388,20 +477,21 @@
         layer_kernel,
         name="layer",
         out_shape=jax.ShapeDtypeStruct((256, 2048), bf16),
-        in_specs=[a, a, a, v, v, a] + [v] * 5 + [a] * 3,
+        in_specs=[a, a, a, v, v, a] + [v] * 3 + [a] * 3,
         out_specs=v,
         scratch_shapes=[
             pltpu.VMEM((2048, 1024), bf16),
             pltpu.VMEM((2048, 1024), bf16),
             pltpu.VMEM((1024, 2048), bf16),
             pltpu.VMEM((256, 2048), f32),
-            pltpu.VMEM((256, 2048), bf16),
-            pltpu.VMEM((16, 64, 2048), bf16),
-            pltpu.VMEM((16, 64, 2048), bf16),
+            pltpu.VMEM((2, 4, 8, 256), f32),
+            pltpu.VMEM((2, 4, 256, 1024), bf16),
+            pltpu.VMEM((2, 4, 4, 64, 1024), bf16),
+            pltpu.VMEM((2, 4, 4, 64, 1024), bf16),
             pltpu.VMEM((256, 1024), bf16),
-            pltpu.VMEM((16, 64, 2048), bf16),
-            pltpu.VMEM((16, 64, 2048), bf16),
-            pltpu.VMEM((256, 2048), f32),
+            pltpu.VMEM((2, 4, 4, 64, 1024), bf16),
+            pltpu.VMEM((2, 4, 4, 64, 1024), bf16),
+            pltpu.VMEM((2, 3, 256, 1024), bf16),
             pltpu.VMEM((16, 192, 256), bf16),
             pltpu.VMEM((4, 4, 256, 128), bf16),
             pltpu.VMEM((4, 4, 384, 128), bf16),
@@ -412,7 +502,9 @@
             pltpu.VMEM((8, 4, 4, 128, 256), bf16),
             dma((3,)),
         ]
-        + [dma((16,))] * 4
+        + [dma((8,))] * 4
+        + [dma((32,))] * 4
+        + [dma((6,))] * 2
         + [dma((4,))] * 9
         + [dma((16,))] * 4
         + [dma((4,))] * 4
@@ -420,7 +512,7 @@
         compiler_params=pltpu.CompilerParams(
             collective_id=1, has_side_effects=True, vmem_limit_bytes=65400 * 1024
         ),
-    )(q_slab, lat_a, lat_b, up_k, up_vt, wo, resid, gain, routes, routes.T, weight, wg, wu, wd)
+    )(q_slab, lat_a, lat_b, up_k, up_vt, wo, resid, gain, told, wg, wu, wd)
 
 
 def shards(
@@ -452,8 +544,11 @@
     key_pack = jnp.concatenate([key_turned[:half], key_turned[half:]], axis=1)
     lat_a = latent_normed[:, :128]
     lat_b = jnp.concatenate([latent_normed[:, 128:], key_pack], axis=0)
+    told = jnp.concatenate(
+        [routes[0].T.astype(jnp.float32), route_weight[0].T, jnp.zeros((4, tokens), jnp.float32)], axis=0
+    )
     return layer(
-        q_slab, lat_a, lat_b, key_up, value_up.T, out_proj, resid[0], norm_gain[None], routes[0], route_weight[0],
+        q_slab, lat_a, lat_b, key_up, value_up.T, out_proj, resid[0], norm_gain[None], told,
         expert_gate[0], expert_up[0], expert_down[0],
     )[None]
 

time: 215 us -> 190 us (0.88); the launches traced: 212 us -> 190 us
  Pallas kernels: 200 us -> 179 us
    pallas_call x1, Pallas kernels: 200 us -> 179 us  [layer(): pl.pallas_call(layer_kernel, name='layer', out_shape=jax.ShapeDtypeStruct...]
    unnamed x17 -> x16, local copies, waits for them, and re-layouts: 5.56 us -> 4.75 us
where the time goes in v4:
time: 190 us
  Pallas kernels  179 us (94%)
  local copies, waits for them, and re-layouts  5.6 us (3%)
  other arithmetic  5 us (3%)
    pallas_call x1, Pallas kernels, layer(): pl.pallas_call(layer_kernel, name='layer', out_shape=jax.ShapeDtypeStruct...  179 us
    unnamed x16, local copies, waits for them, and re-layouts  4.75 us

profile of v4, /device:TPU:0, one launch (start us, length us, event | category | flops | bytes accessed | tf_op | source)
XLA Modules:
  0.0 189.8 jit_solution(12169254367389509508)
XLA Ops:
  0.0 1.2 bitcast_convert_fusion
  1.2 0.9 copy.25
  2.2 0.6 subtract_convert_fusion.1
  2.8 0.1 copy.24
  2.8 0.1 copy.23
  2.9 0.2 subtract_convert_fusion
  3.1 0.0 copy-start.1
  3.1 0.0 copy-start.5
  3.1 0.0 copy-start.2
  3.2 0.0 copy-start.4
  3.2 0.0 copy-start.3
  3.2 0.8 copy.21
  4.0 1.3 pad_maximum_fusion.q_in_hbm
  5.2 0.0 copy-done.1
  5.2 0.1 fusion
  5.4 0.1 fusion.2
  5.5 0.6 fusion.12
  6.1 0.1 fusion.11
  6.2 0.7 fusion.10.lat_b
  6.9 0.7 copy.26
  7.7 0.1 pad.2.clone
  7.8 0.7 maximum_maximum_fusion.told_in
  8.4 179.1 %layer.1 = bf16[256,2048]{1,0:T(8,128)(2,1)} custom-call(bf16[16,192,256]{2,1,0:T(8,128)(2,1)} %pad_maximum_fusion.q_in_hbm, bf16[256,128]{1,0:T(8,128)(2,1)} %get-tuple-element.10.lat_a, bf16[384,128]{1,0:T(8,128)(2,1)} %fusion.10.lat_b, bf16[256,128]{1,0:T(8,128)(2,1)} %up_k.1, bf16[128,256]{1,0:T(8,128)(2,1)} %bitcast.35, bf16[128,256]{1,0:T(8,128)(2,1)} %wo_hbm.1, ...), custom_call_target="tpu_custom_call" | custom-call | tf_op jit(solution)/shard_map/layer/pallas_call | solution.py:476
  187.5 2.3 %copy.28 = bf16[1,256,2048]{2,1,0:T(8,128)(2,1)} copy(bf16[1,256,2048]{2,1,0:T(8,128)(2,1)} %bitcast.32) | data formatting | bytes 2097152
  (13 shorter events, 0.1 us)
Async XLA Ops:
  0.0 3.1 %copy-start = (bf16[1,256,16,128]{3,2,1,0:T(8,128)(2,1)S(1)}, bf16[1,256,16,128]{3,2,1,0:T(8,128)(2,1)}, u32[]{:S(2)}) copy-start(bf16[1,256,16,128]{3,2,1,0:T(8,128)(2,1)} %param.15) | copy-start | bytes 3145732
  3.1 2.2 %copy-start.1 = (bf16[1,256,256]{2,1,0:T(8,128)(2,1)S(1)}, bf16[1,256,256]{2,1,0:T(8,128)(2,1)}, u32[]{:S(2)}) copy-start(bf16[1,256,256]{2,1,0:T(8,128)(2,1)} %param.17) | copy-start | bytes 393220
  3.1 2.3 %copy-start.5 = (f32[256]{0:T(256)S(1)}, f32[256]{0:T(256)}, u32[]{:S(2)}) copy-start(f32[256]{0:T(256)} %param.20) | copy-start | bytes 3076
  3.1 3.8 %copy-start.2 = (bf16[256,128]{1,0:T(8,128)(2,1)S(1)}, bf16[256,128]{1,0:T(8,128)(2,1)}, u32[]{:S(2)}) copy-start(bf16[256,128]{1,0:T(8,128)(2,1)} %param.22) | copy-start | bytes 196612
  3.2 4.5 %copy-start.4 = (s32[1,256,2]{1,2,0:T(2,128)S(1)}, s32[1,256,2]{1,2,0:T(2,128)}, u32[]{:S(2)}) copy-start(s32[1,256,2]{1,2,0:T(2,128)} %param.28) | copy-start | bytes 6148
  3.2 4.6 %copy-start.3 = (f32[1,256,2]{1,2,0:T(2,128)S(1)}, f32[1,256,2]{1,2,0:T(2,128)}, u32[]{:S(2)}) copy-start(f32[1,256,2]{1,2,0:T(2,128)} %param.29) | copy-start | bytes 6148

commit v5 on v4

--- a/solution.py
+++ b/solution.py
@@ -12,33 +12,6 @@
 masked_score = -1e30
 
 
-def rotate(values, positions):
-    half_width = values.shape[-1] // 2
-    frequency = rope_base ** (-jnp.arange(half_width, dtype=jnp.float32) / half_width)
-    angles = positions.astype(jnp.float32)[:, None] * frequency[None, :]
-    cosine = jnp.cos(angles)
-    sine_part = jnp.sin(angles)
-    if values.ndim == 3:
-        cosine = cosine[:, None, :]
-        sine_part = sine_part[:, None, :]
-    floats = values.astype(jnp.float32)
-    first_half = floats[..., :half_width]
-    second_half = floats[..., half_width:]
-    turned = jnp.concatenate(
-        [
-            first_half * cosine - second_half * sine_part,
-            second_half * cosine + first_half * sine_part,
-        ],
-        axis=-1,
-    )
-    return turned.astype(jnp.bfloat16)
-
-
-def rms_scaled(values, gain):
-    floats = values.astype(jnp.float32)
-    return floats * lax.rsqrt(jnp.mean(floats * floats, axis=-1, keepdims=True) + epsilon) * gain
-
-
 ORDER = [(0, 0), (2, 2), (3, 2), (2, 3), (1, 2), (2, 1), (0, 2), (2, 0), (3, 1), (1, 3), (3, 3), (1, 1), (3, 0), (0, 3), (1, 0), (0, 1)]
 MESH = pl.DeviceIdType.MESH
 
@@ -49,6 +22,7 @@
 
 
 PLACE = {0: 0, 1: 1, 3: 2, 2: 3}
+EARLY = 3
 SHIFT = [0, 1, 3, 2]
 PAIRS = [(0, 0), (2, 1), (1, 1), (3, 1), (2, 0), (0, 1), (1, 0), (3, 0)]
 PZ, PJ = packed([o[0] for o in PAIRS]), packed([o[1] for o in PAIRS])
@@ -71,9 +45,9 @@
 
 
 def layer_kernel(
-    q_in_hbm, lat_a, lat_b, up_k, up_vt, wo_hbm, resid, gain, told_in, wg_hbm, wu_hbm, wd_hbm, out,
-    wg, wu, wd, after, told_all, shared, outgoing, arrived, hidden, result, returned, final,
-    q_in, la, lb, keys, vals, attended, heads, wo,
+    nope_t, rope_t, lat_in, lat_gain, key_t, cosine, sine, up_k, up_v, wo_hbm, resid, gain, routes_t, weight_t, wg_hbm, wu_hbm, wd_hbm, out,
+    wg, wu, wd, told_all, shared, outgoing, arrived, hidden, result, returned, final,
+    q_out, q_in, la, lb, up_vt, keys, vals, attended, heads, wo,
     wsem, st, rt, ssh, rsh, sd, rd, sg, rg, sf, rf,
     lsem, sa1, ra1, sb1, rb1, sa2, ra2, sb2, rb2, sq, rq, so, ro, swz, rwz, swy, rwy, swx, rwx, swc, rwc,
 ):
@@ -91,12 +65,6 @@
         pl.semaphore_signal(barrier, inc=1, device_id={"dp": t}, device_id_type=MESH)
     fill_wo = pltpu.make_async_copy(wo_hbm, wo.at[dp, z, y], lsem.at[0])
     fill_wo.start()
-    fill_q = pltpu.make_async_copy(q_in_hbm.at[me], q_in.at[me], lsem.at[1])
-    fill_q.start()
-    fill_a = pltpu.make_async_copy(lat_a, la.at[z, y], lsem.at[2])
-    fill_a.start()
-    fill_b = pltpu.make_async_copy(lat_b, lb.at[z, y], lsem.at[3])
-    fill_b.start()
     loads = [
         pltpu.make_async_copy(a, b, wsem.at[i])
         for i, (a, b) in enumerate(((wg_hbm, wg), (wu_hbm, wu), (wd_hbm, wd)))
@@ -107,14 +75,32 @@
     tok_l = lax.broadcasted_iota(i32, (256, 256), 1)
     upper = jnp.where(tok < tok_l, 1.0, 0.0).astype(bf16)
     expert = lax.broadcasted_iota(i32, (16, 256), 0).astype(f32)
-    hot = [jnp.where(expert == told_in[k : k + 1, :], 1.0, 0.0) for k in range(2)]
+    hot = [jnp.where(expert == routes_t[k : k + 1, :].astype(f32), 1.0, 0.0) for k in range(2)]
     before = jnp.dot((hot[0] + hot[1]).astype(bf16), upper, preferred_element_type=f32) + expert * 64.0
     for h in range(2):
         for k in range(2):
             told_all[h, 0, k : k + 1, :] = jnp.sum(hot[k] * before, axis=0, keepdims=True)
-        told_all[h, 0, 2:8, :] = told_in[2:8, :]
-    fill_a.wait()
-    fill_b.wait()
+        told_all[h, 0, 2:4, :] = weight_t[...]
+        told_all[h, 0, 4:8, :] = jnp.zeros((4, 256), f32)
+
+    lat = lat_in[...].astype(f32)
+    lat = lat * lax.rsqrt(jnp.mean(lat * lat, axis=-1, keepdims=True) + epsilon) * lat_gain[...]
+    la[z, y] = lat[:, 0:128].astype(bf16)
+    lb[z, y, 0:256, :] = lat[:, 128:256].astype(bf16)
+    cos, sin = cosine[...], sine[...]
+    a, b = key_t[0:32, :].astype(f32), key_t[32:64, :].astype(f32)
+    turned = jnp.concatenate([a * cos - b * sin, b * cos + a * sin], axis=0)
+    lb[z, y, 256:384, :] = jnp.concatenate([turned[:, 0:128], turned[:, 128:256]], axis=0).T.astype(bf16)
+    up_vt[...] = up_v[...].astype(f32).T.astype(bf16)
+
+    @pl.loop(0, 16)
+    def _(h):
+        a, b = rope_t[h, 0:32, :].astype(f32), rope_t[h, 32:64, :].astype(f32)
+        q_out[h, 0:128, :] = nope_t[h]
+        q_out[h, 128:160, :] = (a * cosine[...] - b * sine[...]).astype(bf16)
+        q_out[h, 160:192, :] = (b * cosine[...] + a * sine[...]).astype(bf16)
+
+    q_in[me] = q_out[me]
     fill_wo.wait()
     pl.semaphore_wait(barrier, 19)
 
@@ -129,9 +115,27 @@
     a1 = [remote(la.at[z, y], la.at[z, y], sa1.at[d], ra1.at[d], along(d, 0)) for d in (1, 2, 3)]
     b1 = [remote(lb.at[z, y], lb.at[z, y], sb1.at[d], rb1.at[d], along(0, d)) for d in (1, 2, 3)]
     w1 = [remote(wo.at[dp, z, y], wo.at[dp, z, y], swz.at[d], rwz.at[d], along(d, 0)) for d in (1, 2, 3)]
-    a2 = [remote(la.at[:, y], la.at[:, y], sa2.at[d], ra2.at[d], along(0, d)) for d in (1, 2, 3)]
-    b2 = [remote(lb.at[z], lb.at[z], sb2.at[d], rb2.at[d], along(d, 0)) for d in (1, 2, 3)]
-    w2 = [remote(wo.at[dp, :, y], wo.at[dp, :, y], swy.at[d], rwy.at[d], along(0, d)) for d in (1, 2, 3)]
+    ym, yp, yo = [lax.rem(y + n, 4) for n in (3, 1, 2)]
+    zm, zp, zo = [lax.rem(z + n, 4) for n in (3, 1, 2)]
+    up, down, fore, back = along(0, 1), along(0, 3), along(1, 0), along(3, 0)
+    a2 = [
+        remote(la.at[:, y], la.at[:, y], sa2.at[0], ra2.at[0], up),
+        remote(la.at[:, y], la.at[:, y], sa2.at[1], ra2.at[1], down),
+        remote(la.at[0:2, ym], la.at[0:2, ym], sa2.at[2], ra2.at[2], up),
+        remote(la.at[2:4, yp], la.at[2:4, yp], sa2.at[3], ra2.at[3], down),
+    ]
+    b2 = [
+        remote(lb.at[z], lb.at[z], sb2.at[0], rb2.at[0], fore),
+        remote(lb.at[z], lb.at[z], sb2.at[1], rb2.at[1], back),
+        remote(lb.at[zm, 0:2], lb.at[zm, 0:2], sb2.at[2], rb2.at[2], fore),
+        remote(lb.at[zp, 2:4], lb.at[zp, 2:4], sb2.at[3], rb2.at[3], back),
+    ]
+    w2 = [
+        remote(wo.at[dp, :, y], wo.at[dp, :, y], swy.at[0], rwy.at[0], up),
+        remote(wo.at[dp, :, y], wo.at[dp, :, y], swy.at[1], rwy.at[1], down),
+        remote(wo.at[dp, 0:2, ym], wo.at[dp, 0:2, ym], swy.at[2], rwy.at[2], up),
+        remote(wo.at[dp, 2:4, yp], wo.at[dp, 2:4, yp], swy.at[3], rwy.at[3], down),
+    ]
     asks = []
     for r, (dz, dj) in enumerate(PAIRS):
         for e in range(2):
@@ -141,7 +145,7 @@
                     continue
             else:
                 target = lax.rem(z + 4 - dz, 4) * 4 + lax.rem(y // 2 + dj, 2) * 2 + e
-            asks.append(remote(q_in_hbm.at[target], q_in.at[me], sq.at[2 * r + e], rq.at[me], target))
+            asks.append(remote(q_out.at[target], q_in.at[me], sq.at[2 * r + e], rq.at[me], target))
 
     def to_x(g):
         part = wo.at[dp, :, lax.rem(y + 4 - g, 4)]
@@ -165,42 +169,64 @@
         c.start()
     for c in w1:
         c.wait_recv()
-    for c in w2 + to_x(0) + [to_core(0, 0)]:
+    for c in to_x(0) + [to_core(0, 0)]:
         c.start()
     for c in a1:
         c.wait_recv()
-    for c in a2:
+    for c in a2[:2]:
         c.start()
     for c in b1:
         c.wait_recv()
-    for c in b2 + told + asks:
+    for c in b2[:2] + w2[:2] + told + asks[:EARLY]:
         c.start()
-    for g in (1, 2, 3):
-        w2[g - 1].wait_recv()
-        for c in to_x(g) + [to_core(g, 0)]:
-            c.start()
-
     vals[128:144, :] = jnp.ones((16, 4096), bf16)
-    for c in a2 + b2:
-        c.wait_recv()
-
-    @pl.loop(0, 16)
-    def _(b):
-        bz, by = b // 4, lax.rem(b, 4)
-        rows = pl.ds(pl.multiple_of(b * 256, 256), 256)
+
+    def build(bz, by):
+        b = bz * 4 + by
+        start = pl.multiple_of(b * 256, 256)
+        rows = pl.ds(start, 256)
         lat = jnp.concatenate([la[bz, by], lb[bz, by, 0:256, :]], axis=1)
         keys[rows, 0:128] = jnp.dot(lat, up_k[...], preferred_element_type=f32).astype(bf16)
         vals[0:128, rows] = lax.dot_general(
             up_vt[...], lat, (((1,), (1,)), ((), ())), preferred_element_type=f32
         ).astype(bf16)
         turn = lb[bz, by, 256:384, :].astype(f32)
-        swap = pltpu.roll(turn, 64, 1)
-        low = lax.broadcasted_iota(i32, (128, 128), 1) < 64
-        start = pl.multiple_of(b * 256, 256)
-        keys[pl.ds(start, 128), 128:256] = jnp.where(low, turn, swap).astype(bf16)
-        keys[pl.ds(pl.multiple_of(start + 128, 128), 128), 128:256] = jnp.where(low, swap, turn).astype(bf16)
-
-    fill_q.wait()
+        keys[pl.ds(start, 128), 128:256] = turn.astype(bf16)
+        keys[pl.ds(pl.multiple_of(start + 128, 128), 128), 128:256] = pltpu.roll(turn, 64, 1).astype(bf16)
+
+    for n in range(2):
+        a2[n].wait_recv()
+        a2[n + 2].start()
+    for n in range(2):
+        b2[n].wait_recv()
+        b2[n + 2].start()
+    for n in range(2):
+        w2[n].wait_recv()
+        w2[n + 2].start()
+        for c in to_x(2 * n + 1) + [to_core(2 * n + 1, 0)]:
+            c.start()
+    for c in asks[EARLY:]:
+        c.start()
+
+    @pl.loop(0, 9)
+    def _(n):
+        build(lax.rem(z + 3 + n // 3, 4), lax.rem(y + 3 + lax.rem(n, 3), 4))
+
+    for c in a2[2:] + b2[2:]:
+        c.wait_recv()
+
+    @pl.loop(0, 4)
+    def _(n):
+        build(zo, lax.rem(y + n, 4))
+
+    @pl.loop(0, 3)
+    def _(n):
+        build(lax.rem(z + 3 + n, 4), yo)
+
+    for c in w2[2:]:
+        c.wait_recv()
+    for c in to_x(2) + [to_core(2, 0)]:
+        c.start()
     unit = 192.0 ** -0.5 * math.log2(math.e)
     mine = pl.ds(pl.multiple_of(me * 128, 128), 128)
 
@@ -214,9 +240,9 @@
             def _(source=source):
                 remote(q_in.at[source], q_in.at[source], sq.at[0], rq.at[source], source).wait_recv()
 
-        for g in (0, 1, 2):
-
-            @pl.when(r == 2 * g + 2)
+        for i, g in enumerate((0, 1, 3)):
+
+            @pl.when(r == 2 * i + 2)
             def _(g=g):
                 for d in (1, 2, 3):
                     to_x(g)[d - 1].wait_recv()
@@ -272,8 +298,8 @@
 
     lax.fori_loop(0, 8, one_pair, 0)
     for d in (1, 2, 3):
-        to_x(3)[d - 1].wait_recv()
-        to_core(3, d).start()
+        to_x(2)[d - 1].wait_recv()
+        to_core(2, d).start()
     for k in range(1, 16):
         head = along(*ORDER[k])
         there = pl.ds(pl.multiple_of(head * 128, 128), 128)
@@ -286,12 +312,12 @@
     def _(n):
         cols = pl.ds(pl.multiple_of(n * 256, 256), 256)
         p = jnp.dot(heads[...], wo[n].reshape(2048, 256), preferred_element_type=f32).astype(bf16)
-        after[:, cols] = resid[:, cols].astype(f32) + p.astype(f32)
+        out[:, cols] = resid[:, cols].astype(f32) + p.astype(f32)
 
     @pl.loop(0, 8)
     def _(r):
         rows = pl.ds(pl.multiple_of(r * 32, 32), 32)
-        a = after[rows, :]
+        a = out[rows, :]
         scale = lax.rsqrt(jnp.mean(a * a, axis=-1, keepdims=True) + epsilon)
         full = (a * scale * gain[...]).astype(bf16)
         shared[0, 0, rows, :] = full[:, 0:1024]
@@ -436,7 +462,7 @@
                 t = jnp.dot(high, rows, preferred_element_type=f32) + jnp.dot(low, rows, preferred_element_type=f32)
                 if a == 0:
                     wide = slice(h * 1024 + n * 512, h * 1024 + n * 512 + 512)
-                    after[:, wide] = after[:, wide] + t
+                    out[:, wide] = out[:, wide] + t
                 else:
                     shared[h, a, :, cols] = t.astype(bf16)
             if a > 0:
@@ -445,10 +471,10 @@
         for a in (1, 2, 3):
             summed(h, a).wait_recv()
         wide = slice(h * 1024, h * 1024 + 1024)
-        t = after[:, wide]
+        t = out[:, wide]
         for n in range(3):
             t = t + final[h, n].astype(f32)
-        out[:, wide] = t.astype(bf16)
+        out[:, wide] = t
     for h in range(2):
         for a in range(4):
             for d in (1, 2, 3):
@@ -469,21 +495,20 @@
             c.wait_send()
 
 
-def layer(q_slab, lat_a, lat_b, up_k, up_vt, wo, resid, gain, told, wg, wu, wd):
+def layer(nope_t, rope_t, lat, lat_gain, key_t, cos, sin, up_k, up_v, wo, resid, gain, routes_t, weight_t, wg, wu, wd):
     v, a = pl.BlockSpec(memory_space=pltpu.VMEM), pl.BlockSpec(memory_space=pl.ANY)
     bf16, f32 = jnp.bfloat16, jnp.float32
     dma = pltpu.SemaphoreType.DMA
     return pl.pallas_call(
         layer_kernel,
         name="layer",
-        out_shape=jax.ShapeDtypeStruct((256, 2048), bf16),
-        in_specs=[a, a, a, v, v, a] + [v] * 3 + [a] * 3,
+        out_shape=jax.ShapeDtypeStruct((256, 2048), f32),
+        in_specs=[v] * 9 + [a] + [v] * 4 + [a] * 3,
         out_specs=v,
         scratch_shapes=[
             pltpu.VMEM((2048, 1024), bf16),
             pltpu.VMEM((2048, 1024), bf16),
             pltpu.VMEM((1024, 2048), bf16),
-            pltpu.VMEM((256, 2048), f32),
             pltpu.VMEM((2, 4, 8, 256), f32),
             pltpu.VMEM((2, 4, 256, 1024), bf16),
             pltpu.VMEM((2, 4, 4, 64, 1024), bf16),
@@ -493,8 +518,10 @@
             pltpu.VMEM((2, 4, 4, 64, 1024), bf16),
             pltpu.VMEM((2, 3, 256, 1024), bf16),
             pltpu.VMEM((16, 192, 256), bf16),
+            pltpu.VMEM((16, 192, 256), bf16),
             pltpu.VMEM((4, 4, 256, 128), bf16),
             pltpu.VMEM((4, 4, 384, 128), bf16),
+            pltpu.VMEM((128, 256), bf16),
             pltpu.VMEM((4096, 256), bf16),
             pltpu.VMEM((144, 4096), bf16),
             pltpu.VMEM((16, 256, 128), bf16),
@@ -512,7 +539,7 @@
         compiler_params=pltpu.CompilerParams(
             collective_id=1, has_side_effects=True, vmem_limit_bytes=65400 * 1024
         ),
-    )(q_slab, lat_a, lat_b, up_k, up_vt, wo, resid, gain, told, wg, wu, wd)
+    )(nope_t, rope_t, lat, lat_gain, key_t, cos, sin, up_k, up_v, wo, resid, gain, routes_t, weight_t, wg, wu, wd)
 
 
 def shards(
@@ -533,24 +560,15 @@
     route_weight,
 ):
     tokens = latent.shape[1]
-    local_pos = lax.axis_index("sp") * tokens + jnp.arange(tokens, dtype=jnp.int32)
-    latent_normed = rms_scaled(latent[0], latent_gain).astype(jnp.bfloat16)
-    key_turned = rotate(key_rope[0], local_pos)
-    query_turned = rotate(query_rope[0], local_pos)
-    half = tokens // 2
-    q_slab = jnp.concatenate(
-        [query_nope[0].transpose(1, 2, 0), query_turned.transpose(1, 2, 0)], axis=1
-    )
-    key_pack = jnp.concatenate([key_turned[:half], key_turned[half:]], axis=1)
-    lat_a = latent_normed[:, :128]
-    lat_b = jnp.concatenate([latent_normed[:, 128:], key_pack], axis=0)
-    told = jnp.concatenate(
-        [routes[0].T.astype(jnp.float32), route_weight[0].T, jnp.zeros((4, tokens), jnp.float32)], axis=0
-    )
+    positions = lax.axis_index("sp") * tokens + jnp.arange(tokens, dtype=jnp.int32)
+    half_width = key_rope.shape[-1] // 2
+    frequency = rope_base ** (-jnp.arange(half_width, dtype=jnp.float32) / half_width)
+    angles = frequency[:, None] * positions.astype(jnp.float32)[None, :]
     return layer(
-        q_slab, lat_a, lat_b, key_up, value_up.T, out_proj, resid[0], norm_gain[None], told,
-        expert_gate[0], expert_up[0], expert_down[0],
-    )[None]
+        query_nope[0].transpose(1, 2, 0), query_rope[0].transpose(1, 2, 0), latent[0], latent_gain[None],
+        key_rope[0].T, jnp.cos(angles), jnp.sin(angles), key_up, value_up, out_proj, resid[0], norm_gain[None],
+        routes[0].T, route_weight[0].T, expert_gate[0], expert_up[0], expert_down[0],
+    ).astype(jnp.bfloat16)[None]
 
 
 def solution(mesh):

time: 190 us -> 181 us (0.953)
  Pallas kernels: 179 us -> 175 us
  local copies, waits for them, and re-layouts: 5.6 us -> 2.41 us
    pallas_call x1, Pallas kernels: 179 us -> 175 us  [layer(): pl.pallas_call(layer_kernel, name='layer', out_shape=jax.ShapeDtypeStruct...]
    concatenate x4 -> x0, other arithmetic: 2.75 us -> none  [the longest x1 1.26 us: shards(): jnp.concatenate([query_nope[0].transpose(1, 2, 0), query_turned.transpose...]
    broadcast_in_dim x0 -> x1, other arithmetic: none -> 2.71 us  [shards(): layer(query_nope[0].transpose(1, 2, 0), query_rope[0].transpose(1, 2, 0),...]
    unnamed x16 -> x1, local copies, waits for them, and re-layouts: 4.75 us -> 2.41 us
where the time goes in v5:
time: 181 us
  Pallas kernels  175 us (97%)
  other arithmetic  3.57 us (2%)
  local copies, waits for them, and re-layouts  2.41 us (1%)
    pallas_call x1, Pallas kernels, layer(): pl.pallas_call(layer_kernel, name='layer', out_shape=jax.ShapeDtypeStruct...  175 us

profile of v5, /device:TPU:0, one launch (start us, length us, event | category | flops | bytes accessed | tf_op | source)
XLA Modules:
  0.0 180.6 jit_solution(6533930975954492405)
XLA Ops:
  0.0 0.8 multiply_sine_fusion
  0.9 2.4 %copy.16 = bf16[1,256,16,128]{1,3,2,0:T(8,128)(2,1)} copy(bf16[1,256,16,128]{3,2,1,0:T(8,128)(2,1)} %param.15) | data formatting | bytes 2097152 | tf_op args[0]
  3.3 174.7 %layer.1 = f32[256,2048]{1,0:T(8,128)} custom-call(bf16[16,128,256]{2,1,0:T(8,128)(2,1)} %bitcast.27, bf16[16,64,256]{2,1,0:T(8,128)(2,1)} %bitcast.29, bf16[256,256]{1,0:T(8,128)(2,1)} %bitcast.30, f32[1,256]{1,0:T(1,128)} %bitcast.35, bf16[64,256]{1,0:T(8,128)(2,1)} %bitcast.31, f32[32,256]{1,0:T(8,128)} %get-tuple-element.6.cosine, ...), custom_call_target="tpu_custom_call" | custom-call | tf_op jit(solution)/shard_map/layer/pallas_call | solution.py:502
  177.9 2.7 %convert_bitcast_fusion = bf16[1,256,2048]{2,1,0:T(8,128)(2,1)} fusion(f32[256,2048]{1,0:T(8,128)} %layer.1), kind=kLoop, calls=%fused_computation | loop fusion | flops 524288 | bytes 3145728 | tf_op jit(solution)/shard_map/broadcast_in_dim | solution.py:567
  (2 shorter events, 0.0 us)

commit v6 on v5

--- a/solution.py
+++ b/solution.py
@@ -45,7 +45,7 @@
 
 
 def layer_kernel(
-    nope_t, rope_t, lat_in, lat_gain, key_t, cosine, sine, up_k, up_v, wo_hbm, resid, gain, routes_t, weight_t, wg_hbm, wu_hbm, wd_hbm, out,
+    nope, rope_t, lat_in, lat_gain, key_t, cosine, sine, up_k, up_v, wo_hbm, resid, gain, routes_t, weight_t, wg_hbm, wu_hbm, wd_hbm, out,
     wg, wu, wd, told_all, shared, outgoing, arrived, hidden, result, returned, final,
     q_out, q_in, la, lb, up_vt, keys, vals, attended, heads, wo,
     wsem, st, rt, ssh, rsh, sd, rd, sg, rg, sf, rf,
@@ -93,14 +93,6 @@
     lb[z, y, 256:384, :] = jnp.concatenate([turned[:, 0:128], turned[:, 128:256]], axis=0).T.astype(bf16)
     up_vt[...] = up_v[...].astype(f32).T.astype(bf16)
 
-    @pl.loop(0, 16)
-    def _(h):
-        a, b = rope_t[h, 0:32, :].astype(f32), rope_t[h, 32:64, :].astype(f32)
-        q_out[h, 0:128, :] = nope_t[h]
-        q_out[h, 128:160, :] = (a * cosine[...] - b * sine[...]).astype(bf16)
-        q_out[h, 160:192, :] = (b * cosine[...] + a * sine[...]).astype(bf16)
-
-    q_in[me] = q_out[me]
     fill_wo.wait()
     pl.semaphore_wait(barrier, 19)
 
@@ -167,6 +159,18 @@
 
     for c in w1 + a1 + b1:
         c.start()
+    for t in (0, 128):
+        by_head = nope[t : t + 128].astype(f32).transpose(1, 0, 2)
+        for h in range(16):
+            q_out[h, 0:128, t : t + 128] = by_head[h].T.astype(bf16)
+
+    @pl.loop(0, 16)
+    def _(h):
+        a, b = rope_t[h, 0:32, :].astype(f32), rope_t[h, 32:64, :].astype(f32)
+        q_out[h, 128:160, :] = (a * cosine[...] - b * sine[...]).astype(bf16)
+        q_out[h, 160:192, :] = (b * cosine[...] + a * sine[...]).astype(bf16)
+
+    q_in[me] = q_out[me]
     for c in w1:
         c.wait_recv()
     for c in to_x(0) + [to_core(0, 0)]:
@@ -223,10 +227,6 @@
     def _(n):
         build(lax.rem(z + 3 + n, 4), yo)
 
-    for c in w2[2:]:
-        c.wait_recv()
-    for c in to_x(2) + [to_core(2, 0)]:
-        c.start()
     unit = 192.0 ** -0.5 * math.log2(math.e)
     mine = pl.ds(pl.multiple_of(me * 128, 128), 128)
 
@@ -240,9 +240,16 @@
             def _(source=source):
                 remote(q_in.at[source], q_in.at[source], sq.at[0], rq.at[source], source).wait_recv()
 
+        @pl.when(r == 2)
+        def _():
+            for c in w2[2:]:
+                c.wait_recv()
+            for c in to_x(2) + [to_core(2, 0)]:
+                c.start()
+
         for i, g in enumerate((0, 1, 3)):
 
-            @pl.when(r == 2 * i + 2)
+            @pl.when(r == 2 * i + 3)
             def _(g=g):
                 for d in (1, 2, 3):
                     to_x(g)[d - 1].wait_recv()
@@ -495,7 +502,7 @@
             c.wait_send()
 
 
-def layer(nope_t, rope_t, lat, lat_gain, key_t, cos, sin, up_k, up_v, wo, resid, gain, routes_t, weight_t, wg, wu, wd):
+def layer(nope, rope_t, lat, lat_gain, key_t, cos, sin, up_k, up_v, wo, resid, gain, routes_t, weight_t, wg, wu, wd):
     v, a = pl.BlockSpec(memory_space=pltpu.VMEM), pl.BlockSpec(memory_space=pl.ANY)
     bf16, f32 = jnp.bfloat16, jnp.float32
     dma = pltpu.SemaphoreType.DMA
@@ -539,7 +546,7 @@
         compiler_params=pltpu.CompilerParams(
             collective_id=1, has_side_effects=True, vmem_limit_bytes=65400 * 1024
         ),
-    )(nope_t, rope_t, lat, lat_gain, key_t, cos, sin, up_k, up_v, wo, resid, gain, routes_t, weight_t, wg, wu, wd)
+    )(nope, rope_t, lat, lat_gain, key_t, cos, sin, up_k, up_v, wo, resid, gain, routes_t, weight_t, wg, wu, wd)
 
 
 def shards(
@@ -565,7 +572,7 @@
     frequency = rope_base ** (-jnp.arange(half_width, dtype=jnp.float32) / half_width)
     angles = frequency[:, None] * positions.astype(jnp.float32)[None, :]
     return layer(
-        query_nope[0].transpose(1, 2, 0), query_rope[0].transpose(1, 2, 0), latent[0], latent_gain[None],
+        query_nope[0], query_rope[0].transpose(1, 2, 0), latent[0], latent_gain[None],
         key_rope[0].T, jnp.cos(angles), jnp.sin(angles), key_up, value_up, out_proj, resid[0], norm_gain[None],
         routes[0].T, route_weight[0].T, expert_gate[0], expert_up[0], expert_down[0],
     ).astype(jnp.bfloat16)[None]

time: 181 us -> 177 us (0.978)
  Pallas kernels: 175 us -> 172 us
  local copies, waits for them, and re-layouts: 2.41 us -> 0 us
    unnamed x1 -> x0, local copies, waits for them, and re-layouts: 2.41 us -> none
    pallas_call x1, Pallas kernels: 175 us -> 172 us  [layer(): pl.pallas_call(layer_kernel, name='layer', out_shape=jax.ShapeDtypeStruct...]
where the time goes in v6:
time: 177 us; the launch traced here: 176 us
  Pallas kernels  172 us (97%)
  other arithmetic  3.56 us (2%)
    pallas_call x1, Pallas kernels, layer(): pl.pallas_call(layer_kernel, name='layer', out_shape=jax.ShapeDtypeStruct...  172 us

profile of v6, /device:TPU:0, one launch (start us, length us, event | category | flops | bytes accessed | tf_op | source)
XLA Modules:
  0.0 176.0 jit_solution(2960424622842207467)
XLA Ops:
  0.0 0.8 multiply_sine_fusion
  0.8 172.4 %layer.1 = f32[256,2048]{1,0:T(8,128)} custom-call(bf16[256,16,128]{2,1,0:T(8,128)(2,1)} %bitcast.25, bf16[16,64,256]{2,1,0:T(8,128)(2,1)} %bitcast.27, bf16[256,256]{1,0:T(8,128)(2,1)} %bitcast.28, f32[1,256]{1,0:T(1,128)} %bitcast.33, bf16[64,256]{1,0:T(8,128)(2,1)} %bitcast.29, f32[32,256]{1,0:T(8,128)} %get-tuple-element.6.cosine, ...), custom_call_target="tpu_custom_call" | custom-call | tf_op jit(solution)/shard_map/layer/pallas_call | solution.py:509
  173.3 2.7 %convert_bitcast_fusion = bf16[1,256,2048]{2,1,0:T(8,128)(2,1)} fusion(f32[256,2048]{1,0:T(8,128)} %layer.1), kind=kLoop, calls=%fused_computation | loop fusion | flops 524288 | bytes 3145728 | tf_op jit(solution)/shard_map/broadcast_in_dim | solution.py:574
  (2 shorter events, 0.0 us)

commit v7 on v6

--- a/solution.py
+++ b/solution.py
@@ -46,7 +46,7 @@
 
 def layer_kernel(
     nope, rope_t, lat_in, lat_gain, key_t, cosine, sine, up_k, up_v, wo_hbm, resid, gain, routes_t, weight_t, wg_hbm, wu_hbm, wd_hbm, out,
-    wg, wu, wd, told_all, shared, outgoing, arrived, hidden, result, returned, final,
+    wg, wu, wd, told_all, shared, outgoing, arrived, hidden, result, returned, final, halfway,
     q_out, q_in, la, lb, up_vt, keys, vals, attended, heads, wo,
     wsem, st, rt, ssh, rsh, sd, rd, sg, rg, sf, rf,
     lsem, sa1, ra1, sb1, rb1, sa2, ra2, sb2, rb2, sq, rq, so, ro, swz, rwz, swy, rwy, swx, rwx, swc, rwc,
@@ -450,10 +450,15 @@
             c.wait_send()
 
     def summed(h, a):
-        n = 3 * h + a - 1
+        n = 4 * h + a - 1
         return remote(shared.at[h, a], final.at[h, a - 1], sf.at[n], rf.at[n], line(h, 4 - SHIFT[a]))
 
-    for a in (1, 2, 3, 0):
+    def crossing(h, n):
+        at = 4 * h + 2 + n
+        half = shared.at[h, 3, 128 * n : 128 * n + 128]
+        return remote(half, halfway.at[h, n], sf.at[at], rf.at[at], line(h, 1 + 2 * n))
+
+    for a in (3, 1, 2, 0):
         for h in range(2):
             for d in (1, 2, 3):
                 given(h, d, a).wait_recv()
@@ -472,14 +477,24 @@
                     out[:, wide] = out[:, wide] + t
                 else:
                     shared[h, a, :, cols] = t.astype(bf16)
-            if a > 0:
-                summed(h, a).start()
-    for h in range(2):
-        for a in (1, 2, 3):
+            if a == 3:
+                crossing(h, 0).start()
+                crossing(h, 1).start()
+    for h in range(2):
+        for a in (1, 2):
+            crossing(h, 2 - a).wait_recv()
+            rows = slice(128, 256) if a == 1 else slice(0, 128)
+            t = shared[h, a, rows, :].astype(f32) + halfway[h, 2 - a].astype(f32)
+            shared[h, a, rows, :] = t.astype(bf16)
+    for h in range(2):
+        for a in (1, 2):
+            summed(h, a).start()
+    for h in range(2):
+        for a in (1, 2):
             summed(h, a).wait_recv()
         wide = slice(h * 1024, h * 1024 + 1024)
         t = out[:, wide]
-        for n in range(3):
+        for n in range(2):
             t = t + final[h, n].astype(f32)
         out[:, wide] = t
     for h in range(2):
@@ -487,8 +502,9 @@
             for d in (1, 2, 3):
                 dealt(h, d, a).wait_send()
                 given(h, d, a).wait_send()
-        for a in (1, 2, 3):
-            summed(h, a).wait_send()
+        for n in range(2):
+            summed(h, n + 1).wait_send()
+            crossing(h, n).wait_send()
     for c in told + a1 + b1 + w1 + a2 + b2 + w2 + asks:
         c.wait_send()
     for n in range(16):
@@ -523,7 +539,8 @@
             pltpu.VMEM((256, 1024), bf16),
             pltpu.VMEM((2, 4, 4, 64, 1024), bf16),
             pltpu.VMEM((2, 4, 4, 64, 1024), bf16),
-            pltpu.VMEM((2, 3, 256, 1024), bf16),
+            pltpu.VMEM((2, 2, 256, 1024), bf16),
+            pltpu.VMEM((2, 2, 128, 1024), bf16),
             pltpu.VMEM((16, 192, 256), bf16),
             pltpu.VMEM((16, 192, 256), bf16),
             pltpu.VMEM((4, 4, 256, 128), bf16),
@@ -538,7 +555,7 @@
         ]
         + [dma((8,))] * 4
         + [dma((32,))] * 4
-        + [dma((6,))] * 2
+        + [dma((8,))] * 2
         + [dma((4,))] * 9
         + [dma((16,))] * 4
         + [dma((4,))] * 4

time: 177 us -> 176 us (level)
  no operation moved by 1% of the time
where the time goes in v7:
time: 176 us
  Pallas kernels  172 us (98%)
  other arithmetic  3.56 us (2%)
    pallas_call x1, Pallas kernels, layer(): pl.pallas_call(layer_kernel, name='layer', out_shape=jax.ShapeDtypeStruct...  172 us

profile of v7, /device:TPU:0, one launch (start us, length us, event | category | flops | bytes accessed | tf_op | source)
XLA Modules:
  0.0 175.8 jit_solution(2882864031611070208)
XLA Ops:
  0.0 0.8 multiply_sine_fusion
  0.8 172.3 %layer.1 = f32[256,2048]{1,0:T(8,128)} custom-call(bf16[256,16,128]{2,1,0:T(8,128)(2,1)} %bitcast.25, bf16[16,64,256]{2,1,0:T(8,128)(2,1)} %bitcast.27, bf16[256,256]{1,0:T(8,128)(2,1)} %bitcast.28, f32[1,256]{1,0:T(1,128)} %bitcast.33, bf16[64,256]{1,0:T(8,128)(2,1)} %bitcast.29, f32[32,256]{1,0:T(8,128)} %get-tuple-element.6.cosine, ...), custom_call_target="tpu_custom_call" | custom-call | tf_op jit(solution)/shard_map/layer/pallas_call | solution.py:525
  173.1 2.7 %convert_bitcast_fusion = bf16[1,256,2048]{2,1,0:T(8,128)(2,1)} fusion(f32[256,2048]{1,0:T(8,128)} %layer.1), kind=kLoop, calls=%fused_computation | loop fusion | flops 524288 | bytes 3145728 | tf_op jit(solution)/shard_map/broadcast_in_dim | solution.py:591
  (2 shorter events, 0.0 us)
